TPU v7x, 32 devices: a whole 2x2x4 slice. The times are simulated.
32 devices in a mesh: rep: 2 (over y), fs: 4 (over z), tp: 4 (over x, core).
Axes of the slice: x: 2, y: 2, z: 4, core: 2. Of those that a mesh axis runs over, the one named last changes fastest.
Arguments:
- activations: bfloat16 [8, 256, 2048], P(('rep', 'fs'), None, 'tp'), may hold values from -15 to 15
- norm_gain: float32 [2048], replicated, may hold values from 0.1 to 1.9
- w_value: bfloat16 [2048, 2048], P('fs', 'tp'), may hold values from -0.125 to 0.125
- w_gate_conv: bfloat16 [2048, 2048], P('fs', 'tp'), may hold values from -0.125 to 0.125
- conv_weight: float32 [31, 2048], P(None, 'tp'), may hold values from -3 to 3
- chan_gain: float32 [2048], P('tp'), may hold values from 0.1 to 1.9
- w_conv_out: bfloat16 [2048, 2048], P('tp', 'fs'), may hold values from -0.125 to 0.125
- mix_gain: float32 [2048], replicated, may hold values from 0.1 to 1.9
- w_gate: bfloat16 [2048, 3072], P('fs', 'tp'), may hold values from -0.125 to 0.125
- w_up: bfloat16 [2048, 3072], P('fs', 'tp'), may hold values from -0.125 to 0.125
- w_down: bfloat16 [3072, 2048], P('tp', 'fs'), may hold values from -0.109375 to 0.109375
- final_gain: float32 [2048], P('tp'), may hold values from 0.1 to 1.9
Outputs:
- result: bfloat16 [8, 256, 2048], P(('rep', 'fs'), None, 'tp')
All inputs are finite; a program needn't handle non-finite values.
Results may differ from a plain program's by a relative error of at most 0.013.
Values may be sent and summed in bfloat16 or wider, within the bound.
A program may use at most 64 MiB of HBM per device.

v0:
```python
import functools

import jax
import jax.numpy as jnp
from jax import lax
from jax.experimental import pallas as pl
from jax.experimental.pallas import tpu as pltpu
from jax.sharding import PartitionSpec as P

EPS = 1e-06
MESH = pl.DeviceIdType.MESH
F32 = jnp.float32
BF16 = jnp.bfloat16


def remote(src, dst, send, recv, target):
    return pltpu.make_async_remote_copy(
        src_ref=src, dst_ref=dst, send_sem=send, recv_sem=recv, device_id=target, device_id_type=MESH
    )


def chunk_of(extent, want):
    return want if extent % want == 0 else extent


def kernel(
    R, F, T, split, length,
    x_ref, ng_ref, cw_ref, cg_ref, mg_ref, fg_ref,
    wv_ref, wg_ref, wo_ref, wga_ref, wup_ref, wd_ref,
    out_ref,
    bv, bg, bo, bga, bup, bd,
    xg, rows, glu, conv, act, part1, part2, got1, got2, firsts, hid, st1, st2, sg1, sg2,
    own_sem, zs, zr, ys, yr, ts, tr,
):
    f = lax.axis_index("fs")
    me = lax.axis_index("tp")
    rep = lax.axis_index("rep")
    count, dt = x_ref.shape
    width = dt * T
    local = [wv_ref, wg_ref, wo_ref, wga_ref, wup_ref, wd_ref]
    bufs = [bv, bg, bo, bga, bup, bd]

    barrier = pltpu.get_barrier_semaphore()
    greeted = 0
    for target in (lax.rem(f + 1, F), lax.rem(f + F - 1, F)):
        pl.semaphore_signal(barrier, inc=1, device_id={"fs": target}, device_id_type=MESH)
        greeted += 1
    if split == 2:
        pl.semaphore_signal(barrier, inc=1, device_id={"rep": 1 - rep}, device_id_type=MESH)
        greeted += 1
    for d in range(1, T):
        pl.semaphore_signal(barrier, inc=1, device_id={"tp": lax.rem(me + d, T)}, device_id_type=MESH)
        greeted += 1
    own = [
        pltpu.make_async_copy(local[w], bufs[w].at[f], own_sem.at[w]) for w in range(6)
    ]
    for copy in own:
        copy.start()
    pl.semaphore_wait(barrier, greeted)

    def half(w):
        n = local[w].shape[0] // split
        return pl.ds(pl.multiple_of((rep if split == 2 else 0) * n, n), n)

    def other(w):
        n = local[w].shape[0] // split
        return pl.ds(pl.multiple_of((1 - rep) * n, n), n)

    def hop(w, side, s):
        shard = f - s if side == 0 else f + s
        target = f + 1 if side == 0 else f - 1
        src = local[w].at[half(w)] if s == 0 else bufs[w].at[shard, half(w)]
        return remote(src, bufs[w].at[shard, half(w)], zs.at[side, w, s], zr.at[side, w, s + 1], {"fs": target})

    def arrival(w, side, s):
        shard = f - s if side == 0 else f + s
        ref = bufs[w].at[shard, half(w)]
        return remote(ref, ref, zs.at[side, w, s], zr.at[side, w, s], {"fs": f})

    def across(w, side, s):
        shard = f - s if side == 0 else f + s
        ref = bufs[w].at[shard, half(w)]
        return remote(ref, ref, ys.at[side, w, s], yr.at[side, w, s], {"rep": 1 - rep})

    def across_in(w, side, s):
        shard = f - s if side == 0 else f + s
        ref = bufs[w].at[shard, other(w)]
        return remote(ref, ref, ys.at[side, w, s], yr.at[side, w, s], {"rep": 1 - rep})

    def has(side, s):
        return f >= s if side == 0 else f + s <= F - 1

    def sends(side, s):
        ahead = f < F - 1 if side == 0 else f > 0
        return jnp.logical_and(has(side, s), ahead)

    def launch(w):
        for side in (0, 1):
            @pl.when(sends(side, 0))
            def _():
                hop(w, side, 0).start()

    def relay(group, stages=range(1, F)):
        for s in stages:
            for w in group:
                for side in (0, 1):
                    @pl.when(has(side, s))
                    def _():
                        arrival(w, side, s).wait_recv()
                        if s < F - 1:
                            @pl.when(sends(side, s))
                            def _():
                                hop(w, side, s).start()
                        if split == 2:
                            across(w, side, s).start()

    def settle(group):
        for w in group:
            own[w].wait()
        if split == 2:
            for s in range(1, F):
                for w in group:
                    for side in (0, 1):
                        @pl.when(has(side, s))
                        def _():
                            across_in(w, side, s).wait_recv()

    def tp_send(k, src, dst_at, d):
        return remote(src, dst_at, ts.at[k, d], tr.at[k, d], {"tp": lax.rem(me + d, T)})

    for w in (0, 1):
        launch(w)
    for d in range(1, T):
        tp_send(0, x_ref, xg.at[me], d).start()
    launch(2)
    xg[me] = x_ref[...]
    for d in range(1, T):
        peer = lax.rem(me + T - d, T)
        tp_send(0, x_ref, xg.at[peer], d).wait_recv()

    block = chunk_of(count, 16)

    def norm_rows(src, gain):
        def step(i, _):
            r = pl.ds(pl.multiple_of(i * block, block), block)
            vals = [src[t, r, :].astype(F32) for t in range(T)]
            ss = sum(jnp.sum(v * v, axis=1, keepdims=True) for v in vals)
            scale = lax.rsqrt(ss / width + EPS)
            for t in range(T):
                rows[r, t * dt:(t + 1) * dt] = (
                    vals[t] * scale * gain[t:t + 1, :]
                ).astype(BF16)
            return 0
        lax.fori_loop(0, count // block, step, 0)

    norm_rows(xg, ng_ref)
    relay((0, 1, 2))
    for w in (3, 4, 5):
        launch(w)
    settle((0, 1))

    chan = bv.shape[2]
    batch = count // length
    taps = cw_ref.shape[0]
    pad = 8 * ((taps - 1 + 7) // 8)
    lead = pad - (taps - 1)

    def columns(buf, c, n):
        block_w = buf[:, :, pl.ds(pl.multiple_of(c * n, n), n)]
        return block_w.reshape(block_w.shape[0] * block_w.shape[1], n)

    nc = chunk_of(chan, 256)

    def glu_step(c, _):
        value = jnp.dot(rows[...], columns(bv, c, nc), preferred_element_type=F32)
        gate = jnp.dot(rows[...], columns(bg, c, nc), preferred_element_type=F32)
        res = value * jax.nn.sigmoid(gate)
        for b in range(batch):
            glu[b, pl.ds(pad, length), pl.ds(pl.multiple_of(c * nc, nc), nc)] = (
                res[b * length:(b + 1) * length]
            )
        return 0

    for b in range(batch):
        glu[b, 0:pad, :] = jnp.zeros((pad, chan), F32)
        glu[b, pad + length:, :] = jnp.zeros((8, chan), F32)
    lax.fori_loop(0, chan // nc, glu_step, 0)
    relay((3,), (1,))

    lanes = chunk_of(chan, 128)
    span = chunk_of(length, 64)
    strips = chan // lanes

    def conv_step(i, _):
        q = lax.rem(i, strips)
        p = i // strips
        cols = pl.ds(pl.multiple_of(q * lanes, lanes), lanes)
        weights = cw_ref[:, cols]
        for b in range(batch):
            total = jnp.zeros((span, lanes), F32)
            for shift in range(8):
                acc = None
                for tap in range(taps):
                    if (lead + tap) % 8 != shift:
                        continue
                    base = lead + tap - shift
                    term = weights[tap:tap + 1, :] * glu[
                        b, pl.ds(pl.multiple_of(p * span + base, 8), span + 8), cols
                    ]
                    acc = term if acc is None else acc + term
                if acc is not None:
                    total = total + acc[shift:shift + span]
            conv[pl.ds(pl.multiple_of(b * length + p * span, span), span), cols] = total
        return 0

    lax.fori_loop(0, strips * (length // span), conv_step, 0)

    lane = lax.broadcasted_iota(jnp.int32, (count, 128), 1)

    def across_lanes(a, b):
        table = jnp.where(lane == 0, a, jnp.where(lane == 1, b, 0.0))
        return jnp.transpose(table)[0:8, :]

    def down_rows(top):
        full = jnp.concatenate([top, jnp.zeros((120, count), F32)], axis=0)
        return jnp.transpose(full)

    values = conv[...]
    local_sum = jnp.sum(values, axis=1, keepdims=True)
    dev = values - local_sum / chan
    st1[...] = across_lanes(local_sum, jnp.sum(dev * dev, axis=1, keepdims=True))
    sg1[me] = st1[...]
    for d in range(1, T):
        tp_send(1, st1, sg1.at[me], d).start()
    relay((4,), (1,))
    for d in range(1, T):
        peer = lax.rem(me + T - d, T)
        tp_send(1, st1, sg1.at[peer], d).wait_recv()
    sums = [sg1[t] for t in range(T)]
    mean = sum(s[0:1, :] for s in sums) / (chan * T)
    spread = sum(
        s[1:2, :] + chan * (s[0:1, :] / chan - mean) * (s[0:1, :] / chan - mean) for s in sums
    ) / (chan * T)
    inv = lax.rsqrt(spread + EPS)
    line = lax.broadcasted_iota(jnp.int32, (8, count), 0)
    table = down_rows(jnp.where(line == 0, mean, jnp.where(line == 1, inv, 0.0)))
    normed = (conv[...] - table[:, 0:1]) * table[:, 1:2] * cg_ref[...]
    act[...] = (normed * jax.nn.sigmoid(normed)).astype(BF16)

    settle((2,))

    def project(src, buf, part):
        dsh = buf.shape[2]
        for j in range(F):
            t, off = (j * dsh) // dt, (j * dsh) % dt
            prod = jnp.dot(src[...], buf[j], preferred_element_type=F32)
            part[t, :, off:off + dsh] = prod.astype(BF16)

    def scatter(k, part, got):
        for d in range(1, T):
            tp_send(k, part.at[lax.rem(me + d, T)], got.at[d - 1], d).start()

    def gathered(k, part, got):
        total = part[me].astype(F32)
        for d in range(1, T):
            tp_send(k, part.at[me], got.at[d - 1], d).wait_recv()
            total = total + got[d - 1].astype(F32)
        return total

    def piece(t):
        return remote(part2.at[t], got2.at[me], ts.at[4, t], tr.at[4, me], {"tp": t})

    def piece_in(t):
        return remote(part2.at[t], got2.at[t], ts.at[4, t], tr.at[4, t], {"tp": t})

    project(act, bo, part1)
    scatter(2, part1, got1)
    relay((5,), (1,))
    first = (x_ref[...].astype(F32) + gathered(2, part1, got1)).astype(BF16)
    firsts[me] = first
    for d in range(1, T):
        tp_send(3, firsts.at[me], firsts.at[me], d).start()
    relay((3,), (2,))
    for d in range(1, T):
        peer = lax.rem(me + T - d, T)
        tp_send(3, firsts.at[peer], firsts.at[peer], d).wait_recv()
    relay((4,), (2,))
    norm_rows(firsts, mg_ref)
    relay((5,), (2,))
    relay((3, 4), range(3, F))
    settle((3, 4))

    ff = bga.shape[2]
    nf = chunk_of(ff, 256)

    def ff_step(c, _):
        gate = jnp.dot(rows[...], columns(bga, c, nf), preferred_element_type=F32)
        up = jnp.dot(rows[...], columns(bup, c, nf), preferred_element_type=F32)
        hid[:, pl.ds(pl.multiple_of(c * nf, nf), nf)] = (
            gate * jax.nn.sigmoid(gate) * up
        ).astype(BF16)
        return 0

    lax.fori_loop(0, ff // nf, ff_step, 0)
    if F == T and bd.shape[2] == dt:
        def down(shard):
            prod = jnp.dot(hid[...], bd[shard], preferred_element_type=F32)
            part2[shard] = prod.astype(BF16)

            @pl.when(shard != me)
            def _():
                piece(shard).start()

        own[5].wait()
        down(f)
        for s in range(1, F):
            if s >= 3:
                relay((5,), (s,))
            for side in (0, 1):
                @pl.when(has(side, s))
                def _():
                    if split == 2:
                        across_in(5, side, s).wait_recv()
                    down(f - s if side == 0 else f + s)
    else:
        relay((5,), range(3, F))
        settle((5,))
        project(hid, bd, part2)
        for d in range(1, T):
            piece(lax.rem(me + d, T)).start()
    second = firsts[me].astype(F32) + part2[me].astype(F32)
    for d in range(1, T):
        peer = lax.rem(me + d, T)
        piece_in(peer).wait_recv()
        second = second + got2[peer].astype(F32)
    total = jnp.sum(second * second, axis=1, keepdims=True)
    conv[:, 0:dt] = second
    st2[...] = across_lanes(total, total)
    sg2[me] = st2[...]
    for d in range(1, T):
        tp_send(5, st2, sg2.at[me], d).start()
    for d in range(1, T):
        peer = lax.rem(me + T - d, T)
        tp_send(5, st2, sg2.at[peer], d).wait_recv()
    full = sum(sg2[t] for t in range(T))
    table = down_rows(full)
    scale = lax.rsqrt(table[:, 0:1] / width + EPS)
    out_ref[...] = (conv[:, 0:dt] * scale * fg_ref[...]).astype(BF16)

    for w in range(6):
        for side in (0, 1):
            for s in range(F):
                if s < F - 1:
                    @pl.when(sends(side, s))
                    def _():
                        hop(w, side, s).wait_send()
                if s >= 1 and split == 2:
                    @pl.when(has(side, s))
                    def _():
                        across(w, side, s).wait_send()
    for d in range(1, T):
        peer = lax.rem(me + d, T)
        tp_send(0, x_ref, xg.at[me], d).wait_send()
        tp_send(1, st1, sg1.at[me], d).wait_send()
        tp_send(2, part1.at[peer], got1.at[d - 1], d).wait_send()
        tp_send(3, firsts.at[me], firsts.at[me], d).wait_send()
        piece(peer).wait_send()
        tp_send(5, st2, sg2.at[me], d).wait_send()


def body(
    activations, norm_gain, w_value, w_gate_conv, conv_weight, chan_gain,
    w_conv_out, mix_gain, w_gate, w_up, w_down, final_gain,
):
    batch, length, dt = activations.shape
    count = batch * length
    R, F, T = lax.axis_size("rep"), lax.axis_size("fs"), lax.axis_size("tp")
    weights = (w_value, w_gate_conv, w_conv_out, w_gate, w_up, w_down)
    split = 2 if R == 2 and all(w.shape[0] % 32 == 0 for w in weights) else 1
    width = dt * T
    chan, ff = w_value.shape[1], w_gate.shape[1]
    taps = conv_weight.shape[0]
    pad = 8 * ((taps - 1 + 7) // 8)
    vmem, hbm = pl.BlockSpec(memory_space=pltpu.VMEM), pl.BlockSpec(memory_space=pl.ANY)
    ysh = (2, 6, F) if split == 2 else (1,)
    dma = pltpu.SemaphoreType.DMA
    out = pl.pallas_call(
        functools.partial(kernel, R, F, T, split, length),
        out_shape=jax.ShapeDtypeStruct((count, dt), BF16),
        in_specs=[vmem] * 6 + [hbm] * 6,
        out_specs=vmem,
        scratch_shapes=[pltpu.VMEM((F,) + w.shape, BF16) for w in weights] + [
            pltpu.VMEM((T, count, dt), BF16),
            pltpu.VMEM((count, width), BF16),
            pltpu.VMEM((batch, pad + length + 8, chan), F32),
            pltpu.VMEM((count, max(chan, dt)), F32),
            pltpu.VMEM((count, chan), BF16),
            pltpu.VMEM((T, count, dt), BF16),
            pltpu.VMEM((T, count, dt), BF16),
            pltpu.VMEM((T - 1, count, dt), BF16),
            pltpu.VMEM((T, count, dt), BF16),
            pltpu.VMEM((T, count, dt), BF16),
            pltpu.VMEM((count, ff), BF16),
            pltpu.VMEM((8, count), F32),
            pltpu.VMEM((8, count), F32),
            pltpu.VMEM((T, 8, count), F32),
            pltpu.VMEM((T, 8, count), F32),
            dma((6,)),
            dma((2, 6, F)),
            dma((2, 6, F)),
            dma(ysh),
            dma(ysh),
            dma((6, T)),
            dma((6, T)),
        ],
        compiler_params=pltpu.CompilerParams(
            collective_id=0, has_side_effects=True, vmem_limit_bytes=60 * 1024 * 1024
        ),
        name="block",
    )(
        activations.reshape(count, dt),
        norm_gain.reshape(T, dt),
        conv_weight,
        chan_gain.reshape(1, chan),
        mix_gain.reshape(T, dt),
        final_gain.reshape(1, dt),
        *weights,
    )
    return out.reshape(batch, length, dt)


def solution(mesh):
    in_specs = (
        P(("rep", "fs"), None, "tp"),
        P(),
        P("fs", "tp"),
        P("fs", "tp"),
        P(None, "tp"),
        P("tp"),
        P("tp", "fs"),
        P(),
        P("fs", "tp"),
        P("fs", "tp"),
        P("tp", "fs"),
        P("tp"),
    )
    out_specs = P(("rep", "fs"), None, "tp")
    return jax.shard_map(body, mesh=mesh, in_specs=in_specs, out_specs=out_specs, check_vma=False)
```

profile of v0, /device:TPU:0, one launch (start us, length us, event | category | flops | bytes accessed | tf_op | source)
XLA Modules:
  0.0 167.4 jit_solution(5839455191405500891)
XLA Ops:
  0.0 0.0 copy-start
  0.0 1.3 reshape.19.ng_ref
  1.3 0.0 copy-done
  1.3 0.6 reshape.21.mg_ref
  1.9 163.8 %block.1 = bf16[256,512]{1,0:T(8,128)(2,1)} custom-call(bf16[256,512]{1,0:T(8,128)(2,1)} %bitcast.5, f32[4,512]{1,0:T(4,128)} %reshape.19.ng_ref, f32[31,512]{1,0:T(8,128)} %cw_ref.1, f32[1,512]{1,0:T(1,128)} %bitcast.6, f32[4,512]{1,0:T(4,128)} %reshape.21.mg_ref, f32[1,512]{1,0:T(1,128)} %bitcast.7, bf16[512,512]{1,0:T(8,128)(2,1)} %wv_ref.1, ...), custom_call_target="tpu_custom_call" | custom-call | tf_op jit(solution)/shard_map/block/pallas_call | solution.py:387
  165.7 1.7 copy.14
Async XLA Ops:
  0.0 1.3 copy-start
where the time goes:
time: 168 us; the launch traced here: 167 us
  Pallas kernels  164 us (98%)
  local copies, waits for them, and re-layouts  3.59 us (2%)
    pallas_call x1, Pallas kernels, body(): pl.pallas_call(functools.partial(kernel, R, F, T, split, length), out_sha...  164 us

commit v1 on v0

--- a/solution.py
+++ b/solution.py
@@ -23,7 +23,7 @@
     return want if extent % want == 0 else extent
 
 
-def kernel(
+def ring_kernel(
     R, F, T, split, length,
     x_ref, ng_ref, cw_ref, cg_ref, mg_ref, fg_ref,
     wv_ref, wg_ref, wo_ref, wga_ref, wup_ref, wd_ref,
@@ -368,7 +368,611 @@
         tp_send(5, st2, sg2.at[me], d).wait_send()
 
 
-def body(
+CH = 2
+
+
+def fast_kernel(
+    length,
+    x_ref, ng_ref, cw_ref, cg_ref, mg_ref, fg_ref,
+    wv_ref, wg_ref, wo_ref, wga_ref, wup_ref, wd_ref,
+    out_ref,
+    bv, bg, bo, bga, bup, bd,
+    xg, rows, accv, accg, glu, conv, act, part, got, q1, q1in, firsts, hid,
+    part2, got2, q2, q2in, sec, secb, secin, st1, sg1, st2, sg2, fin, finin,
+    own_sem, zs, zr, ms, mr, ys, yr, xos, xor_, ags, agr, sts, str_, rss, rsr, ds_, dr, qs, qr, os_, orr,
+):
+    f = lax.axis_index("fs")
+    me = lax.axis_index("tp")
+    rep = lax.axis_index("rep")
+    count, dt = x_ref.shape
+    T = 4
+    width = dt * T
+    rows_all = 2 * count
+    batch = count // length
+    chan, ff = bv.shape[2], bga.shape[2]
+    local = [wv_ref, wg_ref, wo_ref, wga_ref, wup_ref, wd_ref]
+    bufs = [bv, bg, bo, bga, bup, bd]
+    VAL, GATE, CVO, GA, UP, DOWN = range(6)
+    outer = jnp.logical_or(f == 0, f == 3)
+    near = 1 + f // 3
+    po, pi, fo = 3 * (f - 1), 3 - f, 3 * (2 - f)
+    sib = me + 1 - 2 * lax.rem(me, 2)
+    mir = lax.rem(me + 2, T)
+    dia = lax.rem(sib + 2, T)
+
+    def view(ref, w, h, c):
+        if w == DOWN:
+            n = ref.shape[1] // 2
+            k = n // CH
+            return ref.at[:, pl.ds(pl.multiple_of(h * n + c * k, k), k)]
+        n = ref.shape[0] // 2
+        k = n // CH
+        return ref.at[pl.ds(pl.multiple_of(h * n + c * k, k), k), :]
+
+    barrier = pltpu.get_barrier_semaphore()
+
+    def greet(**target):
+        pl.semaphore_signal(barrier, inc=1, device_id=target, device_id_type=MESH)
+
+    def zsend(w, hs, c):
+        h = rep if hs == 0 else 1 - rep
+        return remote(
+            view(local[w], w, h, c), view(bufs[w].at[f], w, h, c), zs.at[w, hs, c], zr.at[w, hs, c], {"fs": near}
+        )
+
+    def xsend():
+        return remote(x_ref, xg.at[me, 0], xos, xor_, {"fs": near})
+
+    def result_sends():
+        return (
+            remote(secb, secin, os_.at[0], orr.at[0], {"fs": po}),
+            remote(fin, finin, os_.at[1], orr.at[1], {"fs": po}),
+        )
+
+    lane = lax.broadcasted_iota(jnp.int32, (count, 128), 1)
+    line = lax.broadcasted_iota(jnp.int32, (8, count), 0)
+
+    def across_lanes(a, b):
+        table = jnp.where(lane == 0, a, jnp.where(lane == 1, b, 0.0))
+        return jnp.transpose(table)[0:8, :]
+
+    def down_rows(top):
+        full = jnp.concatenate([top, jnp.zeros((120, count), F32)], axis=0)
+        return jnp.transpose(full)
+
+    @pl.when(outer)
+    def _():
+        greet(fs=near)
+        pl.semaphore_wait(barrier, 1)
+        order = [(VAL, 0), (GATE, 0), None, (CVO, 0), (VAL, 1), (GATE, 1), (CVO, 1), (GA, 0), (UP, 0), (GA, 1)]
+        for item in order:
+            if item is None:
+                xsend().start()
+            else:
+                for c in range(CH):
+                    zsend(item[0], item[1], c).start()
+        zsend(DOWN, 0, 0).start()
+        for c in range(CH):
+            zsend(UP, 1, c).start()
+        for c in range(1, CH):
+            zsend(DOWN, 0, c).start()
+        for c in range(CH):
+            zsend(DOWN, 1, c).start()
+        xsend().wait_send()
+        for w in range(6):
+            for hs in range(2):
+                for c in range(CH):
+                    zsend(w, hs, c).wait_send()
+        for r in (remote(secb, secin, os_.at[0], orr.at[0], {"fs": near}),
+                  remote(fin, finin, os_.at[1], orr.at[1], {"fs": near})):
+            r.wait_recv()
+        scale = lax.rsqrt(down_rows(finin[...])[:, 0:1] / width + EPS)
+        out_ref[...] = (secin[...].astype(F32) * scale * fg_ref[...]).astype(BF16)
+
+    @pl.when(jnp.logical_not(outer))
+    def _():
+        greet(fs=po)
+        greet(fs=pi)
+        greet(rep=1 - rep)
+        for t in (sib, mir, dia):
+            greet(tp=t)
+        own = [pltpu.make_async_copy(local[w], bufs[w].at[f], own_sem.at[w]) for w in range(6)]
+        for copy in own:
+            copy.start()
+        pl.semaphore_wait(barrier, 6)
+
+        def arrived(ref, send, recv):
+            remote(ref, ref, send, recv, {"fs": f}).wait_recv()
+
+        def mid_own(w, c):
+            return remote(
+                view(local[w], w, rep, c), view(bufs[w].at[f], w, rep, c), ms.at[w, 0, c], mr.at[w, 0, c], {"fs": pi}
+            )
+
+        def mid_fwd(w, c):
+            ref = view(bufs[w].at[po], w, rep, c)
+            return remote(ref, ref, ms.at[w, 1, c], mr.at[w, 1, c], {"fs": pi})
+
+        def y_fwd(w, k, c):
+            ref = view(bufs[w].at[fo if k else pi], w, rep, c)
+            return remote(ref, ref, ys.at[w, k, c], yr.at[w, k, c], {"rep": 1 - rep})
+
+        def send_own(w):
+            for c in range(CH):
+                mid_own(w, c).start()
+
+        def relay_mid(w, c):
+            arrived(view(bufs[w].at[po], w, rep, c), zs.at[w, 0, c], zr.at[w, 0, c])
+            mid_fwd(w, c).start()
+
+        def relay_y(w, k, c):
+            arrived(view(bufs[w].at[fo if k else pi], w, rep, c), ms.at[w, k, c], mr.at[w, k, c])
+            y_fwd(w, k, c).start()
+
+        def wait_z(w):
+            for c in range(CH):
+                arrived(view(bufs[w].at[po], w, 1 - rep, c), zs.at[w, 1, c], zr.at[w, 1, c])
+
+        def wait_y(w, k):
+            for c in range(CH):
+                arrived(view(bufs[w].at[fo if k else pi], w, 1 - rep, c), ys.at[w, k, c], yr.at[w, k, c])
+
+        def ag(p, buf, slot, kind):
+            ref = buf.at[mir if kind == 2 else me, slot]
+            return remote(ref, ref, ags.at[p, slot, kind], agr.at[p, slot, kind], {"tp": mir if kind == 1 else sib})
+
+        def ag_in(p, buf, slot, kind):
+            ref = buf.at[(sib, mir, dia)[kind], slot]
+            return remote(ref, ref, ags.at[p, slot, kind], agr.at[p, slot, kind], {"tp": me})
+
+        def ag_start(p, buf, slot):
+            ag(p, buf, slot, 1).start()
+            ag(p, buf, slot, 0).start()
+
+        def ag_forward(p, buf, slot):
+            ag_in(p, buf, slot, 1).wait_recv()
+            ag(p, buf, slot, 2).start()
+
+        def ag_finish(p, buf, slot):
+            ag_in(p, buf, slot, 0).wait_recv()
+            ag_in(p, buf, slot, 2).wait_recv()
+
+        block = chunk_of(count, 16)
+
+        def norm_rows(src, slot, gain):
+            def step(i, _):
+                r = pl.ds(pl.multiple_of(i * block, block), block)
+                o = pl.ds(pl.multiple_of(slot * count + i * block, block), block)
+                vals = [src[t, slot, r, :].astype(F32) for t in range(T)]
+                ss = sum(jnp.sum(v * v, axis=1, keepdims=True) for v in vals)
+                scale = lax.rsqrt(ss / width + EPS)
+                for t in range(T):
+                    rows[t, o, :] = (vals[t] * scale * gain[:, t * dt:(t + 1) * dt]).astype(BF16)
+                return 0
+            lax.fori_loop(0, count // block, step, 0)
+
+        def stat(k, slot, src, dst, d):
+            return remote(src, dst, sts.at[k, slot, d], str_.at[k, slot, d], {"tp": lax.rem(me + d, T)})
+
+        def stat_send(k, slot, src, dst):
+            for d in range(1, T):
+                stat(k, slot, src.at[slot], dst.at[slot, me], d).start()
+
+        def stat_wait(k, slot, src, dst):
+            for d in range(1, T):
+                stat(k, slot, src.at[slot], dst.at[slot, lax.rem(me + T - d, T)], d).wait_recv()
+
+        xg[me, 1] = x_ref[...]
+        send_own(VAL)
+        send_own(GATE)
+        remote(x_ref, xg.at[me, 1], ags.at[0, 1, 1], agr.at[0, 1, 1], {"tp": mir}).start()
+        remote(x_ref, xg.at[me, 1], ags.at[0, 1, 0], agr.at[0, 1, 0], {"tp": sib}).start()
+        for c in range(CH):
+            relay_mid(VAL, c)
+            relay_y(VAL, 0, c)
+        ag_forward(0, xg, 1)
+        for c in range(CH):
+            relay_mid(GATE, c)
+            relay_y(GATE, 0, c)
+        send_own(CVO)
+        ag_finish(0, xg, 1)
+        norm_rows(xg, 1, ng_ref)
+        relay_y(VAL, 1, 0)
+        arrived(xg.at[me, 0], xos, xor_)
+        ag_start(0, xg, 0)
+        for c in range(1, CH):
+            relay_y(VAL, 1, c)
+        for c in range(CH):
+            relay_mid(CVO, c)
+            relay_y(GATE, 1, c)
+        send_own(GA)
+        send_own(UP)
+        ag_forward(0, xg, 0)
+        relay_y(CVO, 0, 0)
+        ag_finish(0, xg, 0)
+        norm_rows(xg, 0, ng_ref)
+
+        pad = glu.shape[1] - length - 8
+        taps = cw_ref.shape[0]
+        lead = pad - (taps - 1)
+        nc = chunk_of(chan, 256)
+        for b in range(2 * batch):
+            glu[b, 0:pad, :] = jnp.zeros((pad, chan), F32)
+            glu[b, pad + length:, :] = jnp.zeros((8, chan), F32)
+
+        def s1(shard, first, last):
+            def step(c, _):
+                cols = pl.ds(pl.multiple_of(c * nc, nc), nc)
+                value = jnp.dot(rows[shard], bv[shard, :, cols], preferred_element_type=F32)
+                gate = jnp.dot(rows[shard], bg[shard, :, cols], preferred_element_type=F32)
+                if not first:
+                    value = value + accv[:, cols]
+                    gate = gate + accg[:, cols]
+                if last:
+                    res = value * jax.nn.sigmoid(gate)
+                    for b in range(2 * batch):
+                        glu[b, pl.ds(pad, length), cols] = res[b * length:(b + 1) * length]
+                else:
+                    accv[:, cols] = value
+                    accg[:, cols] = gate
+                return 0
+            lax.fori_loop(0, chan // nc, step, 0)
+
+        own[VAL].wait()
+        own[GATE].wait()
+        s1(f, True, False)
+        wait_y(VAL, 0)
+        wait_y(GATE, 0)
+        s1(pi, False, False)
+        for c in range(1, CH):
+            relay_y(CVO, 0, c)
+        wait_y(VAL, 1)
+        wait_y(GATE, 1)
+        s1(fo, False, False)
+        relay_y(CVO, 1, 0)
+        wait_z(VAL)
+        wait_z(GATE)
+        s1(po, False, True)
+        for c in range(1, CH):
+            relay_y(CVO, 1, c)
+
+        lanes = chunk_of(chan, 128)
+        span = chunk_of(length, 64)
+        strips = chan // lanes
+
+        def convolve(slot):
+            def step(i, _):
+                s = lax.rem(i, strips)
+                p = i // strips
+                cols = pl.ds(pl.multiple_of(s * lanes, lanes), lanes)
+                weights = cw_ref[:, cols]
+                for b in range(batch):
+                    total = jnp.zeros((span, lanes), F32)
+                    for shift in range(8):
+                        acc = None
+                        for tap in range(taps):
+                            if (lead + tap) % 8 != shift:
+                                continue
+                            base = lead + tap - shift
+                            term = weights[tap:tap + 1, :] * glu[
+                                slot * batch + b, pl.ds(pl.multiple_of(p * span + base, 8), span + 8), cols
+                            ]
+                            acc = term if acc is None else acc + term
+                        if acc is not None:
+                            total = total + acc[shift:shift + span]
+                    at = pl.multiple_of(slot * count + b * length + p * span, span)
+                    conv[pl.ds(at, span), cols] = total
+                return 0
+            lax.fori_loop(0, strips * (length // span), step, 0)
+
+        def span_of(slot):
+            return slice(slot * count, (slot + 1) * count)
+
+        def conv_stats(slot):
+            values = conv[span_of(slot), :]
+            local_sum = jnp.sum(values, axis=1, keepdims=True)
+            dev = values - local_sum / chan
+            st1[slot] = across_lanes(local_sum, jnp.sum(dev * dev, axis=1, keepdims=True))
+            sg1[slot, me] = st1[slot]
+            stat_send(0, slot, st1, sg1)
+
+        def activate(slot):
+            stat_wait(0, slot, st1, sg1)
+            sums = [sg1[slot, t] for t in range(T)]
+            mean = sum(s[0:1, :] for s in sums) / (chan * T)
+            spread = sum(
+                s[1:2, :] + chan * (s[0:1, :] / chan - mean) * (s[0:1, :] / chan - mean) for s in sums
+            ) / (chan * T)
+            inv = lax.rsqrt(spread + EPS)
+            table = down_rows(jnp.where(line == 0, mean, jnp.where(line == 1, inv, 0.0)))
+            normed = (conv[span_of(slot), :] - table[:, 0:1]) * table[:, 1:2] * cg_ref[...]
+            act[span_of(slot), :] = (normed * jax.nn.sigmoid(normed)).astype(BF16)
+
+        def rs(slot, kind):
+            if kind == 2:
+                return remote(q1.at[slot], q1in.at[slot], rss.at[slot, 2], rsr.at[slot, 2], {"tp": mir})
+            return remote(
+                part.at[slot, dia if kind else sib], got.at[slot, kind],
+                rss.at[slot, kind], rsr.at[slot, kind], {"tp": sib},
+            )
+
+        def project(slot):
+            def step(j, _):
+                prod = jnp.dot(act[span_of(slot), :], bo[j], preferred_element_type=F32)
+                part[slot, j] = prod.astype(BF16)
+                return 0
+            lax.fori_loop(0, T, step, 0)
+            rs(slot, 1).start()
+            rs(slot, 0).start()
+
+        def pair_sum(slot):
+            rs(slot, 1).wait_recv()
+            q1[slot] = (part[slot, mir].astype(F32) + got[slot, 1].astype(F32)).astype(BF16)
+            rs(slot, 2).start()
+
+        def finish_first(slot):
+            rs(slot, 0).wait_recv()
+            total = xg[me, slot].astype(F32) + (part[slot, me].astype(F32) + got[slot, 0].astype(F32))
+            rs(slot, 2).wait_recv()
+            firsts[me, slot] = (total + q1in[slot].astype(F32)).astype(BF16)
+            ag_start(1, firsts, slot)
+
+        convolve(0)
+        conv_stats(0)
+        relay_y(GA, 0, 0)
+        convolve(1)
+        conv_stats(1)
+        own[CVO].wait()
+        wait_y(CVO, 0)
+        wait_y(CVO, 1)
+        wait_z(CVO)
+        activate(0)
+        project(0)
+        for c in range(1, CH):
+            relay_y(GA, 0, c)
+        activate(1)
+        project(1)
+        pair_sum(0)
+        relay_mid(GA, 0)
+        pair_sum(1)
+        relay_y(UP, 0, 0)
+        for c in range(1, CH):
+            relay_mid(GA, c)
+        finish_first(0)
+        relay_y(UP, 0, 1)
+        relay_mid(UP, 0)
+        relay_y(GA, 1, 0)
+        finish_first(1)
+        ag_forward(1, firsts, 0)
+        for c in range(1, CH):
+            relay_mid(UP, c)
+        send_own(DOWN)
+        for c in range(1, CH):
+            relay_y(GA, 1, c)
+        ag_finish(1, firsts, 0)
+        norm_rows(firsts, 0, mg_ref)
+        ag_forward(1, firsts, 1)
+        relay_y(UP, 1, 0)
+        ag_finish(1, firsts, 1)
+        norm_rows(firsts, 1, mg_ref)
+        for c in range(1, CH):
+            relay_y(UP, 1, c)
+        relay_mid(DOWN, 0)
+        relay_y(DOWN, 0, 0)
+
+        own[GA].wait()
+        own[UP].wait()
+        for w in (GA, UP):
+            wait_y(w, 0)
+            wait_y(w, 1)
+            wait_z(w)
+        nf = chunk_of(ff, 256)
+
+        def ff_step(c, _):
+            cols = pl.ds(pl.multiple_of(c * nf, nf), nf)
+            gate = sum(jnp.dot(rows[t], bga[t, :, cols], preferred_element_type=F32) for t in range(T))
+            up = sum(jnp.dot(rows[t], bup[t, :, cols], preferred_element_type=F32) for t in range(T))
+            hid[:, cols] = (gate * jax.nn.sigmoid(gate) * up).astype(BF16)
+            return 0
+
+        lax.fori_loop(0, ff // nf, ff_step, 0)
+
+        hn = dt // 2
+
+        def hcols(h):
+            return pl.ds(pl.multiple_of(h * hn, hn), hn)
+
+        def pair_send(b, h, n):
+            return remote(part2.at[b, :, hcols(h)], got2.at[b, :, hcols(h)], ds_.at[b, n], dr.at[b, n], {"tp": sib})
+
+        def cross(h, n):
+            return remote(q2.at[:, hcols(h)], q2in.at[:, hcols(h)], qs.at[n], qr.at[n], {"tp": mir})
+
+        def down(b, n):
+            h = rep if n == 0 else 1 - rep
+            prod = jnp.dot(hid[...], bd[b, :, hcols(h)], preferred_element_type=F32)
+            part2[b, :, hcols(h)] = prod.astype(BF16)
+
+            @pl.when(jnp.logical_or(b == sib, b == dia))
+            def _():
+                pair_send(b, h, n).start()
+
+        def combine(b, n):
+            h = rep if n == 0 else 1 - rep
+
+            @pl.when(b == mir)
+            def _():
+                pair_send(b, h, n).wait_recv()
+                q2[:, hcols(h)] = (part2[b, :, hcols(h)].astype(F32) + got2[b, :, hcols(h)].astype(F32)).astype(BF16)
+                cross(h, n).start()
+
+        own[DOWN].wait()
+        down(f, 0)
+        down(f, 1)
+        combine(f, 0)
+        for c in range(1, CH):
+            relay_mid(DOWN, c)
+        down(po, 0)
+        combine(f, 1)
+        for c in range(1, CH):
+            relay_y(DOWN, 0, c)
+        down(pi, 0)
+        combine(po, 0)
+        relay_y(DOWN, 1, 0)
+        wait_y(DOWN, 0)
+        down(pi, 1)
+        combine(pi, 0)
+        for c in range(1, CH):
+            relay_y(DOWN, 1, c)
+        down(fo, 0)
+        combine(pi, 1)
+        wait_z(DOWN)
+        down(po, 1)
+        combine(fo, 0)
+        wait_y(DOWN, 1)
+        down(fo, 1)
+        combine(po, 1)
+        combine(fo, 1)
+
+        for n in range(2):
+            h = rep if n == 0 else 1 - rep
+            pair_send(me, h, n).wait_recv()
+        for n in range(2):
+            h = rep if n == 0 else 1 - rep
+            cross(h, n).wait_recv()
+
+        def finish(slot):
+            r = span_of(slot)
+            second = firsts[me, slot].astype(F32) + part2[me, r, :].astype(F32) + got2[me, r, :].astype(F32)
+            second = second + q2in[r, :].astype(F32)
+            total = jnp.sum(second * second, axis=1, keepdims=True)
+            if slot == 0:
+                secb[...] = second.astype(BF16)
+                result_sends()[0].start()
+            else:
+                sec[...] = second
+            st2[slot] = across_lanes(total, total)
+            sg2[slot, me] = st2[slot]
+            stat_send(1, slot, st2, sg2)
+
+        finish(0)
+        finish(1)
+        stat_wait(1, 0, st2, sg2)
+        fin[...] = sum(sg2[0, t] for t in range(T))
+        result_sends()[1].start()
+        stat_wait(1, 1, st2, sg2)
+        table = down_rows(sum(sg2[1, t] for t in range(T)))
+        scale = lax.rsqrt(table[:, 0:1] / width + EPS)
+        out_ref[...] = (sec[...] * scale * fg_ref[...]).astype(BF16)
+
+        for w in range(6):
+            for c in range(CH):
+                mid_own(w, c).wait_send()
+                mid_fwd(w, c).wait_send()
+                for k in range(2):
+                    y_fwd(w, k, c).wait_send()
+        for slot in range(2):
+            for kind in range(3):
+                ag(0, xg, slot, kind).wait_send()
+                ag(1, firsts, slot, kind).wait_send()
+                rs(slot, kind).wait_send()
+            for d in range(1, T):
+                stat(0, slot, st1.at[slot], sg1.at[slot, me], d).wait_send()
+                stat(1, slot, st2.at[slot], sg2.at[slot, me], d).wait_send()
+        for n in range(2):
+            h = rep if n == 0 else 1 - rep
+            pair_send(sib, h, n).wait_send()
+            pair_send(dia, h, n).wait_send()
+            cross(h, n).wait_send()
+        for r in result_sends():
+            r.wait_send()
+
+
+def fast_body(
+    activations, norm_gain, w_value, w_gate_conv, conv_weight, chan_gain,
+    w_conv_out, mix_gain, w_gate, w_up, w_down, final_gain,
+):
+    batch, length, dt = activations.shape
+    count = batch * length
+    weights = (w_value, w_gate_conv, w_conv_out, w_gate, w_up, w_down)
+    chan, ff = w_value.shape[1], w_gate.shape[1]
+    T = 4
+    pad = 8 * ((conv_weight.shape[0] - 1 + 7) // 8)
+    rows_all = 2 * count
+    vmem, hbm = pl.BlockSpec(memory_space=pltpu.VMEM), pl.BlockSpec(memory_space=pl.ANY)
+    dma = pltpu.SemaphoreType.DMA
+    V = pltpu.VMEM
+    out = pl.pallas_call(
+        functools.partial(fast_kernel, length),
+        out_shape=jax.ShapeDtypeStruct((count, dt), BF16),
+        in_specs=[vmem] * 6 + [hbm] * 6,
+        out_specs=vmem,
+        scratch_shapes=[V((4,) + w.shape, BF16) for w in weights] + [
+            V((T, 2, count, dt), BF16),
+            V((T, rows_all, dt), BF16),
+            V((rows_all, chan), F32),
+            V((rows_all, chan), F32),
+            V((2 * batch, pad + length + 8, chan), F32),
+            V((rows_all, chan), F32),
+            V((rows_all, chan), BF16),
+            V((2, T, count, dt), BF16),
+            V((2, 2, count, dt), BF16),
+            V((2, count, dt), BF16),
+            V((2, count, dt), BF16),
+            V((T, 2, count, dt), BF16),
+            V((rows_all, ff), BF16),
+            V((T, rows_all, dt), BF16),
+            V((T, rows_all, dt), BF16),
+            V((rows_all, dt), BF16),
+            V((rows_all, dt), BF16),
+            V((count, dt), F32),
+            V((count, dt), BF16),
+            V((count, dt), BF16),
+            V((2, 8, count), F32),
+            V((2, T, 8, count), F32),
+            V((2, 8, count), F32),
+            V((2, T, 8, count), F32),
+            V((8, count), F32),
+            V((8, count), F32),
+            dma((6,)),
+            dma((6, 2, CH)),
+            dma((6, 2, CH)),
+            dma((6, 2, CH)),
+            dma((6, 2, CH)),
+            dma((6, 2, CH)),
+            dma((6, 2, CH)),
+            dma(()),
+            dma(()),
+            dma((2, 2, 3)),
+            dma((2, 2, 3)),
+            dma((2, 2, T)),
+            dma((2, 2, T)),
+            dma((2, 3)),
+            dma((2, 3)),
+            dma((T, 2)),
+            dma((T, 2)),
+            dma((2,)),
+            dma((2,)),
+            dma((2,)),
+            dma((2,)),
+        ],
+        compiler_params=pltpu.CompilerParams(
+            collective_id=0, has_side_effects=True, vmem_limit_bytes=60 * 1024 * 1024
+        ),
+        name="block",
+    )(
+        activations.reshape(count, dt),
+        norm_gain.reshape(1, dt * T),
+        conv_weight,
+        chan_gain.reshape(1, chan),
+        mix_gain.reshape(1, dt * T),
+        final_gain.reshape(1, dt),
+        *weights,
+    )
+    return out.reshape(batch, length, dt)
+
+
+def ring_body(
     activations, norm_gain, w_value, w_gate_conv, conv_weight, chan_gain,
     w_conv_out, mix_gain, w_gate, w_up, w_down, final_gain,
 ):
@@ -385,7 +989,7 @@
     ysh = (2, 6, F) if split == 2 else (1,)
     dma = pltpu.SemaphoreType.DMA
     out = pl.pallas_call(
-        functools.partial(kernel, R, F, T, split, length),
+        functools.partial(ring_kernel, R, F, T, split, length),
         out_shape=jax.ShapeDtypeStruct((count, dt), BF16),
         in_specs=[vmem] * 6 + [hbm] * 6,
         out_specs=vmem,
@@ -445,4 +1049,6 @@
         P("tp"),
     )
     out_specs = P(("rep", "fs"), None, "tp")
+    fast = tuple(mesh.shape[a] for a in ("rep", "fs", "tp")) == (2, 4, 4)
+    body = fast_body if fast else ring_body
     return jax.shard_map(body, mesh=mesh, in_specs=in_specs, out_specs=out_specs, check_vma=False)

time: 168 us -> 124 us (0.74)
  Pallas kernels: 164 us -> 123 us
  local copies, waits for them, and re-layouts: 3.59 us -> 1.67 us
    pallas_call x1, Pallas kernels: 164 us -> 123 us  [fast_body(): pl.pallas_call(functools.partial(fast_kernel, length), out_shape=jax.Shap...]
    reshape x2 -> x0, local copies, waits for them, and re-layouts: 1.92 us -> none  [the longest x1 1.31 us: body(): norm_gain.reshape(T, dt)]
where the time goes in v1:
time: 124 us
  Pallas kernels  123 us (99%)
  local copies, waits for them, and re-layouts  1.67 us (1%)
    pallas_call x1, Pallas kernels, fast_body(): pl.pallas_call(functools.partial(fast_kernel, length), out_shape=jax.Shap...  123 us

profile of v1, /device:TPU:0, one launch (start us, length us, event | category | flops | bytes accessed | tf_op | source)
XLA Modules:
  0.0 124.3 jit_solution(13345354233361071982)
XLA Ops:
  0.0 122.6 %block.1 = bf16[256,512]{1,0:T(8,128)(2,1)} custom-call(bf16[256,512]{1,0:T(8,128)(2,1)} %bitcast.7, f32[1,2048]{1,0:T(1,128)} %bitcast.8, f32[31,512]{1,0:T(8,128)} %cw_ref.1, f32[1,512]{1,0:T(1,128)} %bitcast.10, f32[1,2048]{1,0:T(1,128)} %bitcast.9, f32[1,512]{1,0:T(1,128)} %bitcast.11, bf16[512,512]{1,0:T(8,128)(2,1)} %wv_ref.1, ...), custom_call_target="tpu_custom_call" | custom-call | tf_op jit(solution)/shard_map/block/pallas_call | solution.py:905
  122.6 1.7 %copy.14 = bf16[1,256,512]{2,1,0:T(8,128)(2,1)} copy(bf16[1,256,512]{2,1,0:T(8,128)(2,1)} %bitcast.6) | data formatting | bytes 524288

commit v2 on v1

--- a/solution.py
+++ b/solution.py
@@ -368,18 +368,19 @@
         tp_send(5, st2, sg2.at[me], d).wait_send()
 
 
-CH = 2
+PIECES = (2, 2, 2, 2, 2, 4)
+MOST = max(PIECES)
 
 
 def fast_kernel(
     length,
-    x_ref, ng_ref, cw_ref, cg_ref, mg_ref, fg_ref,
+    x_ref, ng_hbm, cw_hbm, cg_hbm, mg_hbm, fg_hbm,
     wv_ref, wg_ref, wo_ref, wga_ref, wup_ref, wd_ref,
     out_ref,
-    bv, bg, bo, bga, bup, bd,
+    ng_ref, cw_ref, cg_ref, mg_ref, fg_ref, bv, bg, bo, bga, bup, bd,
     xg, rows, accv, accg, glu, conv, act, part, got, q1, q1in, firsts, hid,
-    part2, got2, q2, q2in, sec, secb, secin, st1, sg1, st2, sg2, fin, finin,
-    own_sem, zs, zr, ms, mr, ys, yr, xos, xor_, ags, agr, sts, str_, rss, rsr, ds_, dr, qs, qr, os_, orr,
+    accs, part2, got2, q2, q2in, sec, ssq, secb, secin, st1, sg1, st2, sg2, finin,
+    small, own_sem, zs, zr, ms, mr, ys, yr, xos, xor_, ags, agr, sts, str_, rss, rsr, ds_, dr, qs, qr, os_, orr, fs_, fr,
 ):
     f = lax.axis_index("fs")
     me = lax.axis_index("tp")
@@ -402,11 +403,11 @@
 
     def view(ref, w, h, c):
         if w == DOWN:
-            n = ref.shape[1] // 2
-            k = n // CH
-            return ref.at[:, pl.ds(pl.multiple_of(h * n + c * k, k), k)]
+            n, m = ref.shape[1] // 2, ref.shape[0] // 2
+            k = n // 2
+            return ref.at[pl.ds((c % 2) * m, m), pl.ds(pl.multiple_of(h * n + (c // 2) * k, k), k)]
         n = ref.shape[0] // 2
-        k = n // CH
+        k = n // PIECES[w]
         return ref.at[pl.ds(pl.multiple_of(h * n + c * k, k), k), :]
 
     barrier = pltpu.get_barrier_semaphore()
@@ -423,11 +424,25 @@
     def xsend():
         return remote(x_ref, xg.at[me, 0], xos, xor_, {"fs": near})
 
-    def result_sends():
-        return (
-            remote(secb, secin, os_.at[0], orr.at[0], {"fs": po}),
-            remote(fin, finin, os_.at[1], orr.at[1], {"fs": po}),
+    hn = dt // 2
+
+    def half_of(n):
+        return rep if n == 0 else 1 - rep
+
+    def hcols(h):
+        return pl.ds(pl.multiple_of(h * hn, hn), hn)
+
+    def result(n, target):
+        return remote(
+            secb.at[:, hcols(half_of(n))], secin.at[:, hcols(half_of(n))], os_.at[n], orr.at[n], {"fs": target}
         )
+
+    smalls = [
+        pltpu.make_async_copy(src, dst, small.at[k])
+        for k, (src, dst) in enumerate(
+            ((ng_hbm, ng_ref), (cw_hbm, cw_ref), (cg_hbm, cg_ref), (mg_hbm, mg_ref), (fg_hbm, fg_ref))
+        )
+    ]
 
     lane = lax.broadcasted_iota(jnp.int32, (count, 128), 1)
     line = lax.broadcasted_iota(jnp.int32, (8, count), 0)
@@ -442,44 +457,50 @@
 
     @pl.when(outer)
     def _():
-        greet(fs=near)
-        pl.semaphore_wait(barrier, 1)
-        order = [(VAL, 0), (GATE, 0), None, (CVO, 0), (VAL, 1), (GATE, 1), (CVO, 1), (GA, 0), (UP, 0), (GA, 1)]
+        for t in range(T):
+            greet(fs=near, tp=t)
+        smalls[4].start()
+        pl.semaphore_wait(barrier, T)
+        order = [
+            (VAL, 0), (GATE, 0), None, (CVO, 0), (VAL, 1), (GATE, 1), (CVO, 1),
+            (GA, 0), (UP, 0), (GA, 1), (DOWN, 0), (UP, 1), (DOWN, 1),
+        ]
         for item in order:
             if item is None:
                 xsend().start()
             else:
-                for c in range(CH):
+                for c in range(PIECES[item[0]]):
                     zsend(item[0], item[1], c).start()
-        zsend(DOWN, 0, 0).start()
-        for c in range(CH):
-            zsend(UP, 1, c).start()
-        for c in range(1, CH):
-            zsend(DOWN, 0, c).start()
-        for c in range(CH):
-            zsend(DOWN, 1, c).start()
         xsend().wait_send()
         for w in range(6):
             for hs in range(2):
-                for c in range(CH):
+                for c in range(PIECES[w]):
                     zsend(w, hs, c).wait_send()
-        for r in (remote(secb, secin, os_.at[0], orr.at[0], {"fs": near}),
-                  remote(fin, finin, os_.at[1], orr.at[1], {"fs": near})):
-            r.wait_recv()
-        scale = lax.rsqrt(down_rows(finin[...])[:, 0:1] / width + EPS)
+        smalls[4].wait()
+        for n in range(2):
+            result(n, near).wait_recv()
+        for t in range(T):
+            remote(st2.at[0], finin.at[t], fs_.at[t], fr.at[t], {"fs": near}).wait_recv()
+        full = sum(finin[t] for t in range(T))
+        scale = lax.rsqrt(down_rows(full)[:, 0:1] / width + EPS)
         out_ref[...] = (secin[...].astype(F32) * scale * fg_ref[...]).astype(BF16)
 
     @pl.when(jnp.logical_not(outer))
     def _():
-        greet(fs=po)
+        for t in range(T):
+            greet(fs=po, tp=t)
         greet(fs=pi)
         greet(rep=1 - rep)
         for t in (sib, mir, dia):
             greet(tp=t)
         own = [pltpu.make_async_copy(local[w], bufs[w].at[f], own_sem.at[w]) for w in range(6)]
+        load_x = pltpu.make_async_copy(x_ref, xg.at[me, 1], small.at[5])
+        load_x.start()
+        for copy in smalls:
+            copy.start()
         for copy in own:
             copy.start()
-        pl.semaphore_wait(barrier, 6)
+        pl.semaphore_wait(barrier, T + 5)
 
         def arrived(ref, send, recv):
             remote(ref, ref, send, recv, {"fs": f}).wait_recv()
@@ -498,7 +519,7 @@
             return remote(ref, ref, ys.at[w, k, c], yr.at[w, k, c], {"rep": 1 - rep})
 
         def send_own(w):
-            for c in range(CH):
+            for c in range(PIECES[w]):
                 mid_own(w, c).start()
 
         def relay_mid(w, c):
@@ -510,11 +531,11 @@
             y_fwd(w, k, c).start()
 
         def wait_z(w):
-            for c in range(CH):
+            for c in range(PIECES[w]):
                 arrived(view(bufs[w].at[po], w, 1 - rep, c), zs.at[w, 1, c], zr.at[w, 1, c])
 
         def wait_y(w, k):
-            for c in range(CH):
+            for c in range(PIECES[w]):
                 arrived(view(bufs[w].at[fo if k else pi], w, 1 - rep, c), ys.at[w, k, c], yr.at[w, k, c])
 
         def ag(p, buf, slot, kind):
@@ -562,35 +583,37 @@
             for d in range(1, T):
                 stat(k, slot, src.at[slot], dst.at[slot, lax.rem(me + T - d, T)], d).wait_recv()
 
-        xg[me, 1] = x_ref[...]
         send_own(VAL)
         send_own(GATE)
-        remote(x_ref, xg.at[me, 1], ags.at[0, 1, 1], agr.at[0, 1, 1], {"tp": mir}).start()
-        remote(x_ref, xg.at[me, 1], ags.at[0, 1, 0], agr.at[0, 1, 0], {"tp": sib}).start()
-        for c in range(CH):
+        load_x.wait()
+        ag_start(0, xg, 1)
+        for c in range(2):
             relay_mid(VAL, c)
             relay_y(VAL, 0, c)
+        relay_mid(GATE, 0)
         ag_forward(0, xg, 1)
-        for c in range(CH):
-            relay_mid(GATE, c)
-            relay_y(GATE, 0, c)
+        relay_y(GATE, 0, 0)
+        relay_mid(GATE, 1)
+        relay_y(GATE, 0, 1)
         send_own(CVO)
         ag_finish(0, xg, 1)
+        for copy in smalls:
+            copy.wait()
         norm_rows(xg, 1, ng_ref)
         relay_y(VAL, 1, 0)
         arrived(xg.at[me, 0], xos, xor_)
         ag_start(0, xg, 0)
-        for c in range(1, CH):
-            relay_y(VAL, 1, c)
-        for c in range(CH):
-            relay_mid(CVO, c)
-            relay_y(GATE, 1, c)
+        relay_y(VAL, 1, 1)
+        relay_mid(CVO, 0)
+        relay_y(GATE, 1, 0)
+        relay_mid(CVO, 1)
         send_own(GA)
         send_own(UP)
+        relay_y(GATE, 1, 1)
         ag_forward(0, xg, 0)
-        relay_y(CVO, 0, 0)
         ag_finish(0, xg, 0)
         norm_rows(xg, 0, ng_ref)
+        relay_y(CVO, 0, 0)
 
         pad = glu.shape[1] - length - 8
         taps = cw_ref.shape[0]
@@ -624,8 +647,7 @@
         wait_y(VAL, 0)
         wait_y(GATE, 0)
         s1(pi, False, False)
-        for c in range(1, CH):
-            relay_y(CVO, 0, c)
+        relay_y(CVO, 0, 1)
         wait_y(VAL, 1)
         wait_y(GATE, 1)
         s1(fo, False, False)
@@ -633,8 +655,7 @@
         wait_z(VAL)
         wait_z(GATE)
         s1(po, False, True)
-        for c in range(1, CH):
-            relay_y(CVO, 1, c)
+        relay_y(CVO, 1, 1)
 
         lanes = chunk_of(chan, 128)
         span = chunk_of(length, 64)
@@ -719,68 +740,82 @@
 
         convolve(0)
         conv_stats(0)
-        relay_y(GA, 0, 0)
         convolve(1)
         conv_stats(1)
+        relay_y(GA, 0, 0)
         own[CVO].wait()
         wait_y(CVO, 0)
         wait_y(CVO, 1)
         wait_z(CVO)
         activate(0)
         project(0)
-        for c in range(1, CH):
-            relay_y(GA, 0, c)
         activate(1)
+        relay_mid(GA, 0)
         project(1)
         pair_sum(0)
-        relay_mid(GA, 0)
+        relay_y(GA, 0, 1)
         pair_sum(1)
+        relay_mid(GA, 1)
         relay_y(UP, 0, 0)
-        for c in range(1, CH):
-            relay_mid(GA, c)
         finish_first(0)
+        relay_mid(UP, 0)
         relay_y(UP, 0, 1)
-        relay_mid(UP, 0)
+        relay_mid(UP, 1)
+        send_own(DOWN)
         relay_y(GA, 1, 0)
         finish_first(1)
+        relay_y(GA, 1, 1)
         ag_forward(1, firsts, 0)
-        for c in range(1, CH):
-            relay_mid(UP, c)
-        send_own(DOWN)
-        for c in range(1, CH):
-            relay_y(GA, 1, c)
         ag_finish(1, firsts, 0)
         norm_rows(firsts, 0, mg_ref)
+        relay_y(UP, 1, 0)
         ag_forward(1, firsts, 1)
-        relay_y(UP, 1, 0)
+        relay_y(UP, 1, 1)
         ag_finish(1, firsts, 1)
         norm_rows(firsts, 1, mg_ref)
-        for c in range(1, CH):
-            relay_y(UP, 1, c)
         relay_mid(DOWN, 0)
         relay_y(DOWN, 0, 0)
 
+        nf = chunk_of(ff, 256)
+
+        def s5(w, shard, first, last=False):
+            def step(c, _):
+                cols = pl.ds(pl.multiple_of(c * nf, nf), nf)
+                value = jnp.dot(rows[shard], bufs[w][shard, :, cols], preferred_element_type=F32)
+                if not first:
+                    value = value + accs[w - GA, :, cols]
+                if last:
+                    gate = accs[0, :, cols]
+                    hid[:, cols] = (gate * jax.nn.sigmoid(gate) * value).astype(BF16)
+                else:
+                    accs[w - GA, :, cols] = value
+                return 0
+            lax.fori_loop(0, ff // nf, step, 0)
+
         own[GA].wait()
         own[UP].wait()
-        for w in (GA, UP):
-            wait_y(w, 0)
-            wait_y(w, 1)
-            wait_z(w)
-        nf = chunk_of(ff, 256)
-
-        def ff_step(c, _):
-            cols = pl.ds(pl.multiple_of(c * nf, nf), nf)
-            gate = sum(jnp.dot(rows[t], bga[t, :, cols], preferred_element_type=F32) for t in range(T))
-            up = sum(jnp.dot(rows[t], bup[t, :, cols], preferred_element_type=F32) for t in range(T))
-            hid[:, cols] = (gate * jax.nn.sigmoid(gate) * up).astype(BF16)
-            return 0
-
-        lax.fori_loop(0, ff // nf, ff_step, 0)
-
-        hn = dt // 2
-
-        def hcols(h):
-            return pl.ds(pl.multiple_of(h * hn, hn), hn)
+        wait_y(GA, 0)
+        wait_y(GA, 1)
+        wait_z(GA)
+        wait_y(UP, 0)
+        s5(GA, f, True)
+        relay_mid(DOWN, 1)
+        s5(GA, pi, False)
+        relay_mid(DOWN, 2)
+        relay_y(DOWN, 0, 1)
+        s5(GA, po, False)
+        s5(GA, fo, False)
+        relay_mid(DOWN, 3)
+        s5(UP, f, True)
+        s5(UP, pi, False)
+        relay_y(DOWN, 0, 2)
+        wait_y(UP, 1)
+        s5(UP, fo, False)
+        relay_y(DOWN, 0, 3)
+        relay_y(DOWN, 1, 0)
+        wait_z(UP)
+        s5(UP, po, False, True)
+        relay_y(DOWN, 1, 1)
 
         def pair_send(b, h, n):
             return remote(part2.at[b, :, hcols(h)], got2.at[b, :, hcols(h)], ds_.at[b, n], dr.at[b, n], {"tp": sib})
@@ -789,7 +824,7 @@
             return remote(q2.at[:, hcols(h)], q2in.at[:, hcols(h)], qs.at[n], qr.at[n], {"tp": mir})
 
         def down(b, n):
-            h = rep if n == 0 else 1 - rep
+            h = half_of(n)
             prod = jnp.dot(hid[...], bd[b, :, hcols(h)], preferred_element_type=F32)
             part2[b, :, hcols(h)] = prod.astype(BF16)
 
@@ -798,7 +833,7 @@
                 pair_send(b, h, n).start()
 
         def combine(b, n):
-            h = rep if n == 0 else 1 - rep
+            h = half_of(n)
 
             @pl.when(b == mir)
             def _():
@@ -806,67 +841,71 @@
                 q2[:, hcols(h)] = (part2[b, :, hcols(h)].astype(F32) + got2[b, :, hcols(h)].astype(F32)).astype(BF16)
                 cross(h, n).start()
 
+        def outer_stat(d):
+            return remote(
+                st2.at[0], finin.at[me], fs_.at[d], fr.at[me], {"fs": po, "tp": lax.rem(me + d, T)}
+            )
+
+        def finish(n):
+            h = half_of(n)
+            pair_send(me, h, n).wait_recv()
+            cross(h, n).wait_recv()
+            cols = hcols(h)
+            for slot in range(2):
+                r = span_of(slot)
+                second = firsts[me, slot, :, cols].astype(F32) + part2[me, r, cols].astype(F32)
+                second = second + got2[me, r, cols].astype(F32) + q2in[r, cols].astype(F32)
+                if slot == 0:
+                    secb[:, cols] = second.astype(BF16)
+                    result(n, po).start()
+                else:
+                    sec[:, cols] = second
+                total = jnp.sum(second * second, axis=1, keepdims=True)
+                if n == 0:
+                    ssq[r, :] = total
+                    continue
+                total = total + ssq[r, :]
+                st2[slot] = across_lanes(total, total)
+                if slot == 0:
+                    for d in range(T):
+                        outer_stat(d).start()
+                else:
+                    sg2[me] = st2[1]
+                    for d in range(1, T):
+                        stat(1, 1, st2.at[1], sg2.at[me], d).start()
+
         own[DOWN].wait()
         down(f, 0)
         down(f, 1)
+        relay_y(DOWN, 1, 2)
         combine(f, 0)
-        for c in range(1, CH):
-            relay_mid(DOWN, c)
         down(po, 0)
         combine(f, 1)
-        for c in range(1, CH):
-            relay_y(DOWN, 0, c)
         down(pi, 0)
         combine(po, 0)
-        relay_y(DOWN, 1, 0)
         wait_y(DOWN, 0)
         down(pi, 1)
         combine(pi, 0)
-        for c in range(1, CH):
-            relay_y(DOWN, 1, c)
+        relay_y(DOWN, 1, 3)
         down(fo, 0)
         combine(pi, 1)
+        combine(fo, 0)
         wait_z(DOWN)
         down(po, 1)
-        combine(fo, 0)
+        combine(po, 1)
         wait_y(DOWN, 1)
         down(fo, 1)
-        combine(po, 1)
+        finish(0)
         combine(fo, 1)
-
-        for n in range(2):
-            h = rep if n == 0 else 1 - rep
-            pair_send(me, h, n).wait_recv()
-        for n in range(2):
-            h = rep if n == 0 else 1 - rep
-            cross(h, n).wait_recv()
-
-        def finish(slot):
-            r = span_of(slot)
-            second = firsts[me, slot].astype(F32) + part2[me, r, :].astype(F32) + got2[me, r, :].astype(F32)
-            second = second + q2in[r, :].astype(F32)
-            total = jnp.sum(second * second, axis=1, keepdims=True)
-            if slot == 0:
-                secb[...] = second.astype(BF16)
-                result_sends()[0].start()
-            else:
-                sec[...] = second
-            st2[slot] = across_lanes(total, total)
-            sg2[slot, me] = st2[slot]
-            stat_send(1, slot, st2, sg2)
-
-        finish(0)
         finish(1)
-        stat_wait(1, 0, st2, sg2)
-        fin[...] = sum(sg2[0, t] for t in range(T))
-        result_sends()[1].start()
-        stat_wait(1, 1, st2, sg2)
-        table = down_rows(sum(sg2[1, t] for t in range(T)))
+        for d in range(1, T):
+            stat(1, 1, st2.at[1], sg2.at[lax.rem(me + T - d, T)], d).wait_recv()
+        table = down_rows(sum(sg2[t] for t in range(T)))
         scale = lax.rsqrt(table[:, 0:1] / width + EPS)
         out_ref[...] = (sec[...] * scale * fg_ref[...]).astype(BF16)
 
         for w in range(6):
-            for c in range(CH):
+            for c in range(PIECES[w]):
                 mid_own(w, c).wait_send()
                 mid_fwd(w, c).wait_send()
                 for k in range(2):
@@ -878,14 +917,16 @@
                 rs(slot, kind).wait_send()
             for d in range(1, T):
                 stat(0, slot, st1.at[slot], sg1.at[slot, me], d).wait_send()
-                stat(1, slot, st2.at[slot], sg2.at[slot, me], d).wait_send()
         for n in range(2):
-            h = rep if n == 0 else 1 - rep
+            h = half_of(n)
             pair_send(sib, h, n).wait_send()
             pair_send(dia, h, n).wait_send()
             cross(h, n).wait_send()
-        for r in result_sends():
-            r.wait_send()
+            result(n, po).wait_send()
+        for d in range(T):
+            outer_stat(d).wait_send()
+        for d in range(1, T):
+            stat(1, 1, st2.at[1], sg2.at[me], d).wait_send()
 
 
 def fast_body(
@@ -905,9 +946,15 @@
     out = pl.pallas_call(
         functools.partial(fast_kernel, length),
         out_shape=jax.ShapeDtypeStruct((count, dt), BF16),
-        in_specs=[vmem] * 6 + [hbm] * 6,
+        in_specs=[hbm] * 12,
         out_specs=vmem,
-        scratch_shapes=[V((4,) + w.shape, BF16) for w in weights] + [
+        scratch_shapes=[
+            V((1, dt * T), F32),
+            V(conv_weight.shape, F32),
+            V((1, chan), F32),
+            V((1, dt * T), F32),
+            V((1, dt), F32),
+        ] + [V((4,) + w.shape, BF16) for w in weights] + [
             V((T, 2, count, dt), BF16),
             V((T, rows_all, dt), BF16),
             V((rows_all, chan), F32),
@@ -921,26 +968,28 @@
             V((2, count, dt), BF16),
             V((T, 2, count, dt), BF16),
             V((rows_all, ff), BF16),
+            V((2, rows_all, ff), F32),
             V((T, rows_all, dt), BF16),
             V((T, rows_all, dt), BF16),
             V((rows_all, dt), BF16),
             V((rows_all, dt), BF16),
             V((count, dt), F32),
+            V((rows_all, 1), F32),
             V((count, dt), BF16),
             V((count, dt), BF16),
             V((2, 8, count), F32),
             V((2, T, 8, count), F32),
             V((2, 8, count), F32),
-            V((2, T, 8, count), F32),
-            V((8, count), F32),
-            V((8, count), F32),
+            V((T, 8, count), F32),
+            V((T, 8, count), F32),
             dma((6,)),
-            dma((6, 2, CH)),
-            dma((6, 2, CH)),
-            dma((6, 2, CH)),
-            dma((6, 2, CH)),
-            dma((6, 2, CH)),
-            dma((6, 2, CH)),
+            dma((6,)),
+            dma((6, 2, MOST)),
+            dma((6, 2, MOST)),
+            dma((6, 2, MOST)),
+            dma((6, 2, MOST)),
+            dma((6, 2, MOST)),
+            dma((6, 2, MOST)),
             dma(()),
             dma(()),
             dma((2, 2, 3)),
@@ -955,6 +1004,8 @@
             dma((2,)),
             dma((2,)),
             dma((2,)),
+            dma((T,)),
+            dma((T,)),
         ],
         compiler_params=pltpu.CompilerParams(
             collective_id=0, has_side_effects=True, vmem_limit_bytes=60 * 1024 * 1024

time: 124 us -> 117 us (0.944)
  Pallas kernels: 123 us -> 115 us
    pallas_call x1, Pallas kernels: 123 us -> 115 us  [fast_body(): pl.pallas_call(functools.partial(fast_kernel, length), out_shape=jax.Shap...]
where the time goes in v2:
time: 117 us
  Pallas kernels  115 us (98%)
  local copies, waits for them, and re-layouts  1.67 us (1%)
    pallas_call x1, Pallas kernels, fast_body(): pl.pallas_call(functools.partial(fast_kernel, length), out_shape=jax.Shap...  115 us

profile of v2, /device:TPU:0, one launch (start us, length us, event | category | flops | bytes accessed | tf_op | source)
XLA Modules:
  0.0 116.7 jit_solution(9439192402842668180)
XLA Ops:
  0.0 115.0 %block.1 = bf16[256,512]{1,0:T(8,128)(2,1)} custom-call(bf16[256,512]{1,0:T(8,128)(2,1)} %bitcast.7, f32[1,2048]{1,0:T(1,128)} %bitcast.8, f32[31,512]{1,0:T(8,128)} %cw_hbm.1, f32[1,512]{1,0:T(1,128)} %bitcast.10, f32[1,2048]{1,0:T(1,128)} %bitcast.9, f32[1,512]{1,0:T(1,128)} %bitcast.11, bf16[512,512]{1,0:T(8,128)(2,1)} %wv_ref.1, ...), custom_call_target="tpu_custom_call" | custom-call | tf_op jit(solution)/shard_map/block/pallas_call | solution.py:946
  115.0 1.7 %copy.14 = bf16[1,256,512]{2,1,0:T(8,128)(2,1)} copy(bf16[1,256,512]{2,1,0:T(8,128)(2,1)} %bitcast.6) | data formatting | bytes 524288

commit v3 on v2

--- a/solution.py
+++ b/solution.py
@@ -369,7 +369,8 @@
 
 
 PIECES = (2, 2, 2, 2, 2, 4)
-MOST = max(PIECES)
+FIRST = tuple(sum(PIECES[:w]) for w in range(6))
+GROUP = (0, 0, 0, 1, 1, 2)
 
 
 def fast_kernel(
@@ -380,7 +381,7 @@
     ng_ref, cw_ref, cg_ref, mg_ref, fg_ref, bv, bg, bo, bga, bup, bd,
     xg, rows, accv, accg, glu, conv, act, part, got, q1, q1in, firsts, hid,
     accs, part2, got2, q2, q2in, sec, ssq, secb, secin, st1, sg1, st2, sg2, finin,
-    small, own_sem, zs, zr, ms, mr, ys, yr, xos, xor_, ags, agr, sts, str_, rss, rsr, ds_, dr, qs, qr, os_, orr, fs_, fr,
+    small, own_sem, zs, zr, zr2, ms, mr, md, ys, yr, xos, xor_, ags, agr, sts, str_, rss, rsr, ds_, dr, qs, qr, os_, orr, fs_, fr,
 ):
     f = lax.axis_index("fs")
     me = lax.axis_index("tp")
@@ -417,25 +418,25 @@
 
     def zsend(w, hs, c):
         h = rep if hs == 0 else 1 - rep
-        return remote(
-            view(local[w], w, h, c), view(bufs[w].at[f], w, h, c), zs.at[w, hs, c], zr.at[w, hs, c], {"fs": near}
-        )
+        sem = zr2.at[w] if hs else zr.at[FIRST[w] + c]
+        return remote(view(local[w], w, h, c), view(bufs[w].at[f], w, h, c), zs.at[GROUP[w]], sem, {"fs": near})
+
+    def all_sent(sems, extra=1):
+        for g, ref in enumerate((bufs[VAL].at[0:3], bufs[GA].at[0:2], bufs[DOWN].at[0, :, 0:bd.shape[2] * extra // 4])):
+            remote(ref, ref, sems.at[g], sems.at[g], {"fs": f}).wait_send()
 
     def xsend():
         return remote(x_ref, xg.at[me, 0], xos, xor_, {"fs": near})
 
     hn = dt // 2
 
-    def half_of(n):
-        return rep if n == 0 else 1 - rep
-
-    def hcols(h):
-        return pl.ds(pl.multiple_of(h * hn, hn), hn)
-
-    def result(n, target):
-        return remote(
-            secb.at[:, hcols(half_of(n))], secin.at[:, hcols(half_of(n))], os_.at[n], orr.at[n], {"fs": target}
-        )
+    def ucols(j):
+        if j == 0:
+            return pl.ds(pl.multiple_of(rep * hn, hn), hn)
+        return pl.ds(pl.multiple_of((1 - rep) * hn + (j - 1) * (hn // 2), hn // 2), hn // 2)
+
+    def result(cols, target):
+        return remote(secb.at[:, cols], secin.at[:, cols], os_, orr, {"fs": target})
 
     smalls = [
         pltpu.make_async_copy(src, dst, small.at[k])
@@ -463,7 +464,7 @@
         pl.semaphore_wait(barrier, T)
         order = [
             (VAL, 0), (GATE, 0), None, (CVO, 0), (VAL, 1), (GATE, 1), (CVO, 1),
-            (GA, 0), (UP, 0), (GA, 1), (DOWN, 0), (UP, 1), (DOWN, 1),
+            (GA, 0), (UP, 0), (GA, 1), (UP, 1), (DOWN, 0), (DOWN, 1),
         ]
         for item in order:
             if item is None:
@@ -472,15 +473,10 @@
                 for c in range(PIECES[item[0]]):
                     zsend(item[0], item[1], c).start()
         xsend().wait_send()
-        for w in range(6):
-            for hs in range(2):
-                for c in range(PIECES[w]):
-                    zsend(w, hs, c).wait_send()
+        all_sent(zs, 4)
         smalls[4].wait()
-        for n in range(2):
-            result(n, near).wait_recv()
-        for t in range(T):
-            remote(st2.at[0], finin.at[t], fs_.at[t], fr.at[t], {"fs": near}).wait_recv()
+        remote(secb, secin, os_, orr, {"fs": near}).wait_recv()
+        remote(finin, finin, fs_, fr, {"fs": near}).wait_recv()
         full = sum(finin[t] for t in range(T))
         scale = lax.rsqrt(down_rows(full)[:, 0:1] / width + EPS)
         out_ref[...] = (secin[...].astype(F32) * scale * fg_ref[...]).astype(BF16)
@@ -507,56 +503,73 @@
 
         def mid_own(w, c):
             return remote(
-                view(local[w], w, rep, c), view(bufs[w].at[f], w, rep, c), ms.at[w, 0, c], mr.at[w, 0, c], {"fs": pi}
+                view(local[w], w, rep, c), view(bufs[w].at[f], w, rep, c), ms.at[GROUP[w]], mr.at[0, FIRST[w] + c], {"fs": pi}
             )
 
         def mid_fwd(w, c):
             ref = view(bufs[w].at[po], w, rep, c)
-            return remote(ref, ref, ms.at[w, 1, c], mr.at[w, 1, c], {"fs": pi})
+            return remote(ref, ref, ms.at[GROUP[w]], mr.at[1, FIRST[w] + c], {"fs": pi})
+
+        def mid_direct(c):
+            return remote(
+                view(local[DOWN], DOWN, 1 - rep, c), view(bufs[DOWN].at[f], DOWN, 1 - rep, c), md.at[0], md.at[1], {"fs": pi}
+            )
 
         def y_fwd(w, k, c):
             ref = view(bufs[w].at[fo if k else pi], w, rep, c)
-            return remote(ref, ref, ys.at[w, k, c], yr.at[w, k, c], {"rep": 1 - rep})
+            sem = yr.at[k, w + c // 2 if w == DOWN else w]
+            return remote(ref, ref, ys.at[GROUP[w]], sem, {"rep": 1 - rep})
 
         def send_own(w):
             for c in range(PIECES[w]):
                 mid_own(w, c).start()
 
         def relay_mid(w, c):
-            arrived(view(bufs[w].at[po], w, rep, c), zs.at[w, 0, c], zr.at[w, 0, c])
+            arrived(view(bufs[w].at[po], w, rep, c), zs.at[GROUP[w]], zr.at[FIRST[w] + c])
             mid_fwd(w, c).start()
 
+        def wait_mid(w, k, c):
+            arrived(view(bufs[w].at[fo if k else pi], w, rep, c), ms.at[GROUP[w]], mr.at[k, FIRST[w] + c])
+
         def relay_y(w, k, c):
-            arrived(view(bufs[w].at[fo if k else pi], w, rep, c), ms.at[w, k, c], mr.at[w, k, c])
+            wait_mid(w, k, c)
             y_fwd(w, k, c).start()
 
+        def other(w, shard):
+            if w == DOWN:
+                return bufs[w].at[shard, :, pl.ds(pl.multiple_of((1 - rep) * hn, hn), hn)]
+            n = bufs[w].shape[1] // 2
+            return bufs[w].at[shard, pl.ds(pl.multiple_of((1 - rep) * n, n), n), :]
+
         def wait_z(w):
-            for c in range(PIECES[w]):
-                arrived(view(bufs[w].at[po], w, 1 - rep, c), zs.at[w, 1, c], zr.at[w, 1, c])
+            arrived(other(w, po), zs.at[GROUP[w]], zr2.at[w])
 
         def wait_y(w, k):
-            for c in range(PIECES[w]):
-                arrived(view(bufs[w].at[fo if k else pi], w, 1 - rep, c), ys.at[w, k, c], yr.at[w, k, c])
+            arrived(other(w, fo if k else pi), ys.at[GROUP[w]], yr.at[k, w])
+
+        def wait_y_down(k, j):
+            ref = bufs[DOWN].at[fo if k else pi, :, ucols(j)]
+            arrived(ref, ys.at[2], yr.at[k, DOWN + j - 1])
+
+        def wait_direct():
+            arrived(bufs[DOWN].at[pi, :, ucols(2)], md.at[0], md.at[1])
 
         def ag(p, buf, slot, kind):
             ref = buf.at[mir if kind == 2 else me, slot]
-            return remote(ref, ref, ags.at[p, slot, kind], agr.at[p, slot, kind], {"tp": mir if kind == 1 else sib})
-
-        def ag_in(p, buf, slot, kind):
-            ref = buf.at[(sib, mir, dia)[kind], slot]
-            return remote(ref, ref, ags.at[p, slot, kind], agr.at[p, slot, kind], {"tp": me})
+            return remote(
+                ref, ref, ags.at[p, slot], agr.at[p, slot, 1 if kind == 1 else 0], {"tp": mir if kind == 1 else sib}
+            )
 
         def ag_start(p, buf, slot):
             ag(p, buf, slot, 1).start()
             ag(p, buf, slot, 0).start()
 
         def ag_forward(p, buf, slot):
-            ag_in(p, buf, slot, 1).wait_recv()
+            arrived(buf.at[mir, slot], ags.at[p, slot], agr.at[p, slot, 1])
             ag(p, buf, slot, 2).start()
 
         def ag_finish(p, buf, slot):
-            ag_in(p, buf, slot, 0).wait_recv()
-            ag_in(p, buf, slot, 2).wait_recv()
+            arrived(buf.at[0:2, slot], ags.at[p, slot], agr.at[p, slot, 0])
 
         block = chunk_of(count, 16)
 
@@ -572,16 +585,8 @@
                 return 0
             lax.fori_loop(0, count // block, step, 0)
 
-        def stat(k, slot, src, dst, d):
-            return remote(src, dst, sts.at[k, slot, d], str_.at[k, slot, d], {"tp": lax.rem(me + d, T)})
-
-        def stat_send(k, slot, src, dst):
-            for d in range(1, T):
-                stat(k, slot, src.at[slot], dst.at[slot, me], d).start()
-
-        def stat_wait(k, slot, src, dst):
-            for d in range(1, T):
-                stat(k, slot, src.at[slot], dst.at[slot, lax.rem(me + T - d, T)], d).wait_recv()
+        def stat(k, src, dst, d):
+            return remote(src, dst, sts.at[k], str_.at[k], {"tp": lax.rem(me + d, T)})
 
         send_own(VAL)
         send_own(GATE)
@@ -695,10 +700,11 @@
             dev = values - local_sum / chan
             st1[slot] = across_lanes(local_sum, jnp.sum(dev * dev, axis=1, keepdims=True))
             sg1[slot, me] = st1[slot]
-            stat_send(0, slot, st1, sg1)
+            for d in range(1, T):
+                stat(slot, st1.at[slot], sg1.at[slot, me], d).start()
 
         def activate(slot):
-            stat_wait(0, slot, st1, sg1)
+            arrived(sg1.at[slot, 0:3], sts.at[slot], str_.at[slot])
             sums = [sg1[slot, t] for t in range(T)]
             mean = sum(s[0:1, :] for s in sums) / (chan * T)
             spread = sum(
@@ -711,10 +717,9 @@
 
         def rs(slot, kind):
             if kind == 2:
-                return remote(q1.at[slot], q1in.at[slot], rss.at[slot, 2], rsr.at[slot, 2], {"tp": mir})
+                return remote(q1.at[slot], q1in.at[slot], rss.at[slot], rsr.at[slot, 0], {"tp": mir})
             return remote(
-                part.at[slot, dia if kind else sib], got.at[slot, kind],
-                rss.at[slot, kind], rsr.at[slot, kind], {"tp": sib},
+                part.at[slot, dia if kind else sib], got.at[slot, kind], rss.at[slot], rsr.at[slot, kind], {"tp": sib}
             )
 
         def project(slot):
@@ -732,9 +737,8 @@
             rs(slot, 2).start()
 
         def finish_first(slot):
-            rs(slot, 0).wait_recv()
+            arrived(part.at[slot, 0:2], rss.at[slot], rsr.at[slot, 0])
             total = xg[me, slot].astype(F32) + (part[slot, me].astype(F32) + got[slot, 0].astype(F32))
-            rs(slot, 2).wait_recv()
             firsts[me, slot] = (total + q1in[slot].astype(F32)).astype(BF16)
             ag_start(1, firsts, slot)
 
@@ -766,29 +770,27 @@
         finish_first(1)
         relay_y(GA, 1, 1)
         ag_forward(1, firsts, 0)
+        relay_y(UP, 1, 0)
         ag_finish(1, firsts, 0)
         norm_rows(firsts, 0, mg_ref)
-        relay_y(UP, 1, 0)
         ag_forward(1, firsts, 1)
         relay_y(UP, 1, 1)
         ag_finish(1, firsts, 1)
+        relay_y(DOWN, 0, 0)
         norm_rows(firsts, 1, mg_ref)
-        relay_mid(DOWN, 0)
-        relay_y(DOWN, 0, 0)
+        relay_y(DOWN, 0, 1)
 
         nf = chunk_of(ff, 256)
 
-        def s5(w, shard, first, last=False):
+        def s5(w, keep):
             def step(c, _):
                 cols = pl.ds(pl.multiple_of(c * nf, nf), nf)
-                value = jnp.dot(rows[shard], bufs[w][shard, :, cols], preferred_element_type=F32)
-                if not first:
-                    value = value + accs[w - GA, :, cols]
-                if last:
-                    gate = accs[0, :, cols]
+                value = sum(jnp.dot(rows[t], bufs[w][t, :, cols], preferred_element_type=F32) for t in range(T))
+                if keep:
+                    accs[:, cols] = value
+                else:
+                    gate = accs[:, cols]
                     hid[:, cols] = (gate * jax.nn.sigmoid(gate) * value).astype(BF16)
-                else:
-                    accs[w - GA, :, cols] = value
                 return 0
             lax.fori_loop(0, ff // nf, step, 0)
 
@@ -797,74 +799,61 @@
         wait_y(GA, 0)
         wait_y(GA, 1)
         wait_z(GA)
+        s5(GA, True)
+        relay_mid(DOWN, 0)
         wait_y(UP, 0)
-        s5(GA, f, True)
+        wait_z(UP)
+        wait_y(UP, 1)
+        s5(UP, False)
         relay_mid(DOWN, 1)
-        s5(GA, pi, False)
-        relay_mid(DOWN, 2)
-        relay_y(DOWN, 0, 1)
-        s5(GA, po, False)
-        s5(GA, fo, False)
-        relay_mid(DOWN, 3)
-        s5(UP, f, True)
-        s5(UP, pi, False)
-        relay_y(DOWN, 0, 2)
-        wait_y(UP, 1)
-        s5(UP, fo, False)
-        relay_y(DOWN, 0, 3)
-        relay_y(DOWN, 1, 0)
-        wait_z(UP)
-        s5(UP, po, False, True)
-        relay_y(DOWN, 1, 1)
-
-        def pair_send(b, h, n):
-            return remote(part2.at[b, :, hcols(h)], got2.at[b, :, hcols(h)], ds_.at[b, n], dr.at[b, n], {"tp": sib})
-
-        def cross(h, n):
-            return remote(q2.at[:, hcols(h)], q2in.at[:, hcols(h)], qs.at[n], qr.at[n], {"tp": mir})
-
-        def down(b, n):
-            h = half_of(n)
-            prod = jnp.dot(hid[...], bd[b, :, hcols(h)], preferred_element_type=F32)
-            part2[b, :, hcols(h)] = prod.astype(BF16)
+
+        def pair_send(b, j):
+            ref = part2.at[b, :, ucols(j)]
+            return remote(ref, got2.at[b, :, ucols(j)], ds_, dr.at[lax.rem(b // 2 + me // 2, 2), j], {"tp": sib})
+
+        def cross(j):
+            return remote(q2.at[:, ucols(j)], q2in.at[:, ucols(j)], qs, qr.at[j], {"tp": mir})
+
+        def down(b, j):
+            cols = ucols(j)
+            prod = jnp.dot(hid[...], bd[b, :, cols], preferred_element_type=F32)
+            part2[b, :, cols] = prod.astype(BF16)
 
             @pl.when(jnp.logical_or(b == sib, b == dia))
             def _():
-                pair_send(b, h, n).start()
-
-        def combine(b, n):
-            h = half_of(n)
+                pair_send(b, j).start()
+
+        def combine(b, j):
+            cols = ucols(j)
 
             @pl.when(b == mir)
             def _():
-                pair_send(b, h, n).wait_recv()
-                q2[:, hcols(h)] = (part2[b, :, hcols(h)].astype(F32) + got2[b, :, hcols(h)].astype(F32)).astype(BF16)
-                cross(h, n).start()
+                pair_send(b, j).wait_recv()
+                q2[:, cols] = (part2[b, :, cols].astype(F32) + got2[b, :, cols].astype(F32)).astype(BF16)
+                cross(j).start()
 
         def outer_stat(d):
-            return remote(
-                st2.at[0], finin.at[me], fs_.at[d], fr.at[me], {"fs": po, "tp": lax.rem(me + d, T)}
-            )
-
-        def finish(n):
-            h = half_of(n)
-            pair_send(me, h, n).wait_recv()
-            cross(h, n).wait_recv()
-            cols = hcols(h)
+            return remote(st2.at[0], finin.at[me], fs_, fr, {"fs": po, "tp": lax.rem(me + d, T)})
+
+        def finish(j):
+            pair_send(me, j).wait_recv()
+            cross(j).wait_recv()
+            cols = ucols(j)
             for slot in range(2):
                 r = span_of(slot)
                 second = firsts[me, slot, :, cols].astype(F32) + part2[me, r, cols].astype(F32)
                 second = second + got2[me, r, cols].astype(F32) + q2in[r, cols].astype(F32)
                 if slot == 0:
                     secb[:, cols] = second.astype(BF16)
-                    result(n, po).start()
+                    result(cols, po).start()
                 else:
                     sec[:, cols] = second
                 total = jnp.sum(second * second, axis=1, keepdims=True)
-                if n == 0:
+                if j > 0:
+                    total = total + ssq[r, :]
+                if j < 2:
                     ssq[r, :] = total
                     continue
-                total = total + ssq[r, :]
                 st2[slot] = across_lanes(total, total)
                 if slot == 0:
                     for d in range(T):
@@ -872,61 +861,72 @@
                 else:
                     sg2[me] = st2[1]
                     for d in range(1, T):
-                        stat(1, 1, st2.at[1], sg2.at[me], d).start()
+                        stat(2, st2.at[1], sg2.at[me], d).start()
 
         own[DOWN].wait()
+        wait_mid(DOWN, 0, 2)
+        wait_mid(DOWN, 0, 3)
+        down(pi, 0)
         down(f, 0)
+        relay_mid(DOWN, 2)
+        combine(pi, 0)
+        relay_y(DOWN, 1, 0)
+        combine(f, 0)
+        wait_y_down(0, 1)
+        down(pi, 1)
         down(f, 1)
+        relay_mid(DOWN, 3)
+        mid_direct(2).start()
+        mid_direct(3).start()
+        combine(pi, 1)
+        relay_y(DOWN, 1, 1)
+        combine(f, 1)
+        down(po, 0)
+        down(f, 2)
         relay_y(DOWN, 1, 2)
-        combine(f, 0)
-        down(po, 0)
-        combine(f, 1)
-        down(pi, 0)
         combine(po, 0)
-        wait_y(DOWN, 0)
-        down(pi, 1)
-        combine(pi, 0)
+        combine(f, 2)
+        wait_y_down(1, 1)
+        down(fo, 1)
         relay_y(DOWN, 1, 3)
         down(fo, 0)
-        combine(pi, 1)
+        combine(fo, 1)
         combine(fo, 0)
         wait_z(DOWN)
         down(po, 1)
+        down(po, 2)
         combine(po, 1)
-        wait_y(DOWN, 1)
-        down(fo, 1)
+        wait_direct()
+        down(pi, 2)
+        wait_y_down(1, 2)
+        down(fo, 2)
+        combine(po, 2)
+        combine(pi, 2)
+        combine(fo, 2)
         finish(0)
-        combine(fo, 1)
         finish(1)
-        for d in range(1, T):
-            stat(1, 1, st2.at[1], sg2.at[lax.rem(me + T - d, T)], d).wait_recv()
+        finish(2)
+        arrived(sg2.at[0:3], sts.at[2], str_.at[2])
         table = down_rows(sum(sg2[t] for t in range(T)))
         scale = lax.rsqrt(table[:, 0:1] / width + EPS)
         out_ref[...] = (sec[...] * scale * fg_ref[...]).astype(BF16)
 
-        for w in range(6):
-            for c in range(PIECES[w]):
-                mid_own(w, c).wait_send()
-                mid_fwd(w, c).wait_send()
-                for k in range(2):
-                    y_fwd(w, k, c).wait_send()
+        def sent(ref, sem):
+            remote(ref, ref, sem, sem, {"fs": f}).wait_send()
+
+        all_sent(ms, 4)
+        all_sent(ys, 3)
+        sent(bufs[DOWN].at[f, :, ucols(2)], md.at[0])
         for slot in range(2):
-            for kind in range(3):
-                ag(0, xg, slot, kind).wait_send()
-                ag(1, firsts, slot, kind).wait_send()
-                rs(slot, kind).wait_send()
-            for d in range(1, T):
-                stat(0, slot, st1.at[slot], sg1.at[slot, me], d).wait_send()
-        for n in range(2):
-            h = half_of(n)
-            pair_send(sib, h, n).wait_send()
-            pair_send(dia, h, n).wait_send()
-            cross(h, n).wait_send()
-            result(n, po).wait_send()
-        for d in range(T):
-            outer_stat(d).wait_send()
-        for d in range(1, T):
-            stat(1, 1, st2.at[1], sg2.at[me], d).wait_send()
+            sent(xg.at[0:3, slot], ags.at[0, slot])
+            sent(firsts.at[0:3, slot], ags.at[1, slot])
+            sent(part.at[slot, 0:3], rss.at[slot])
+            sent(sg1.at[slot, 0:3], sts.at[slot])
+        sent(sg2.at[0:3], sts.at[2])
+        sent(part2.at[0:2], ds_)
+        sent(q2, qs)
+        sent(secb, os_)
+        sent(finin, fs_)
 
 
 def fast_body(
@@ -968,7 +968,7 @@
             V((2, count, dt), BF16),
             V((T, 2, count, dt), BF16),
             V((rows_all, ff), BF16),
-            V((2, rows_all, ff), F32),
+            V((rows_all, ff), F32),
             V((T, rows_all, dt), BF16),
             V((T, rows_all, dt), BF16),
             V((rows_all, dt), BF16),
@@ -984,28 +984,30 @@
             V((T, 8, count), F32),
             dma((6,)),
             dma((6,)),
-            dma((6, 2, MOST)),
-            dma((6, 2, MOST)),
-            dma((6, 2, MOST)),
-            dma((6, 2, MOST)),
-            dma((6, 2, MOST)),
-            dma((6, 2, MOST)),
+            dma((3,)),
+            dma((sum(PIECES),)),
+            dma((6,)),
+            dma((3,)),
+            dma((2, sum(PIECES))),
+            dma((2,)),
+            dma((3,)),
+            dma((2, 7)),
             dma(()),
             dma(()),
-            dma((2, 2, 3)),
-            dma((2, 2, 3)),
-            dma((2, 2, T)),
-            dma((2, 2, T)),
+            dma((2, 2)),
+            dma((2, 2, 2)),
+            dma((3,)),
+            dma((3,)),
+            dma((2,)),
+            dma((2, 2)),
+            dma(()),
             dma((2, 3)),
-            dma((2, 3)),
-            dma((T, 2)),
-            dma((T, 2)),
-            dma((2,)),
-            dma((2,)),
-            dma((2,)),
-            dma((2,)),
-            dma((T,)),
-            dma((T,)),
+            dma(()),
+            dma((3,)),
+            dma(()),
+            dma(()),
+            dma(()),
+            dma(()),
         ],
         compiler_params=pltpu.CompilerParams(
             collective_id=0, has_side_effects=True, vmem_limit_bytes=60 * 1024 * 1024

time: 117 us -> 113 us (0.966)
  Pallas kernels: 115 us -> 111 us
    pallas_call x1, Pallas kernels: 115 us -> 111 us  [fast_body(): pl.pallas_call(functools.partial(fast_kernel, length), out_shape=jax.Shap...]
where the time goes in v3:
time: 113 us
  Pallas kernels  111 us (98%)
  local copies, waits for them, and re-layouts  1.67 us (1%)
    pallas_call x1, Pallas kernels, fast_body(): pl.pallas_call(functools.partial(fast_kernel, length), out_shape=jax.Shap...  111 us

profile of v3, /device:TPU:0, one launch (start us, length us, event | category | flops | bytes accessed | tf_op | source)
XLA Modules:
  0.0 112.9 jit_solution(10742877135231973112)
XLA Ops:
  0.0 111.2 %block.1 = bf16[256,512]{1,0:T(8,128)(2,1)} custom-call(bf16[256,512]{1,0:T(8,128)(2,1)} %bitcast.7, f32[1,2048]{1,0:T(1,128)} %bitcast.8, f32[31,512]{1,0:T(8,128)} %cw_hbm.1, f32[1,512]{1,0:T(1,128)} %bitcast.10, f32[1,2048]{1,0:T(1,128)} %bitcast.9, f32[1,512]{1,0:T(1,128)} %bitcast.11, bf16[512,512]{1,0:T(8,128)(2,1)} %wv_ref.1, ...), custom_call_target="tpu_custom_call" | custom-call | tf_op jit(solution)/shard_map/block/pallas_call | solution.py:946
  111.2 1.7 %copy.14 = bf16[1,256,512]{2,1,0:T(8,128)(2,1)} copy(bf16[1,256,512]{2,1,0:T(8,128)(2,1)} %bitcast.6) | data formatting | bytes 524288

commit v4 on v3

--- a/solution.py
+++ b/solution.py
@@ -418,11 +418,12 @@
 
     def zsend(w, hs, c):
         h = rep if hs == 0 else 1 - rep
-        sem = zr2.at[w] if hs else zr.at[FIRST[w] + c]
+        sem = zr2.at[w + c // 2 if w == DOWN else w] if hs else zr.at[FIRST[w] + c]
         return remote(view(local[w], w, h, c), view(bufs[w].at[f], w, h, c), zs.at[GROUP[w]], sem, {"fs": near})
 
-    def all_sent(sems, extra=1):
-        for g, ref in enumerate((bufs[VAL].at[0:3], bufs[GA].at[0:2], bufs[DOWN].at[0, :, 0:bd.shape[2] * extra // 4])):
+    def all_sent(sems, eighths):
+        n = bd.shape[1] * eighths // 8
+        for g, ref in enumerate((bufs[VAL].at[0:3], bufs[GA].at[0:2], bufs[DOWN].at[0, 0:n, :])):
             remote(ref, ref, sems.at[g], sems.at[g], {"fs": f}).wait_send()
 
     def xsend():
@@ -433,7 +434,10 @@
     def ucols(j):
         if j == 0:
             return pl.ds(pl.multiple_of(rep * hn, hn), hn)
-        return pl.ds(pl.multiple_of((1 - rep) * hn + (j - 1) * (hn // 2), hn // 2), hn // 2)
+        return pl.ds(pl.multiple_of((1 - rep) * hn + min(j - 1, 1) * (hn // 2), hn // 2), hn // 2)
+
+    def urows(j):
+        return slice(0, rows_all) if j < 2 else slice((j - 2) * count, (j - 1) * count)
 
     def result(cols, target):
         return remote(secb.at[:, cols], secin.at[:, cols], os_, orr, {"fs": target})
@@ -470,10 +474,10 @@
             if item is None:
                 xsend().start()
             else:
-                for c in range(PIECES[item[0]]):
+                for c in range(1 if item == (DOWN, 1) else 0, PIECES[item[0]]):
                     zsend(item[0], item[1], c).start()
         xsend().wait_send()
-        all_sent(zs, 4)
+        all_sent(zs, 7)
         smalls[4].wait()
         remote(secb, secin, os_, orr, {"fs": near}).wait_recv()
         remote(finin, finin, fs_, fr, {"fs": near}).wait_recv()
@@ -520,6 +524,17 @@
             sem = yr.at[k, w + c // 2 if w == DOWN else w]
             return remote(ref, ref, ys.at[GROUP[w]], sem, {"rep": 1 - rep})
 
+        def y_outer():
+            ref = view(bufs[DOWN].at[po], DOWN, rep, 0)
+            return remote(ref, ref, ys.at[2], yr.at[0, 6], {"rep": 1 - rep})
+
+        def wait_z_down(j):
+            if j == 1:
+                arrived(view(bufs[DOWN].at[po], DOWN, 1 - rep, 0), ys.at[2], yr.at[0, 6])
+                arrived(view(bufs[DOWN].at[po], DOWN, 1 - rep, 1), zs.at[2], zr2.at[DOWN])
+            else:
+                arrived(bufs[DOWN].at[po, :, ucols(2)], zs.at[2], zr2.at[DOWN + 1])
+
         def send_own(w):
             for c in range(PIECES[w]):
                 mid_own(w, c).start()
@@ -536,8 +551,6 @@
             y_fwd(w, k, c).start()
 
         def other(w, shard):
-            if w == DOWN:
-                return bufs[w].at[shard, :, pl.ds(pl.multiple_of((1 - rep) * hn, hn), hn)]
             n = bufs[w].shape[1] // 2
             return bufs[w].at[shard, pl.ds(pl.multiple_of((1 - rep) * n, n), n), :]
 
@@ -801,111 +814,132 @@
         wait_z(GA)
         s5(GA, True)
         relay_mid(DOWN, 0)
+        y_outer().start()
         wait_y(UP, 0)
         wait_z(UP)
         wait_y(UP, 1)
         s5(UP, False)
-        relay_mid(DOWN, 1)
 
         def pair_send(b, j):
-            ref = part2.at[b, :, ucols(j)]
-            return remote(ref, got2.at[b, :, ucols(j)], ds_, dr.at[lax.rem(b // 2 + me // 2, 2), j], {"tp": sib})
+            at = (b, urows(j), ucols(j))
+            return remote(part2.at[at], got2.at[at], ds_, dr.at[lax.rem(b // 2 + me // 2, 2), j], {"tp": sib})
 
         def cross(j):
-            return remote(q2.at[:, ucols(j)], q2in.at[:, ucols(j)], qs, qr.at[j], {"tp": mir})
+            at = (urows(j), ucols(j))
+            return remote(q2.at[at], q2in.at[at], qs, qr.at[j], {"tp": mir})
 
         def down(b, j):
-            cols = ucols(j)
-            prod = jnp.dot(hid[...], bd[b, :, cols], preferred_element_type=F32)
-            part2[b, :, cols] = prod.astype(BF16)
+            r, cols = urows(j), ucols(j)
+            prod = jnp.dot(hid[r, :], bd[b, :, cols], preferred_element_type=F32)
+            part2[b, r, cols] = prod.astype(BF16)
 
             @pl.when(jnp.logical_or(b == sib, b == dia))
             def _():
                 pair_send(b, j).start()
 
         def combine(b, j):
-            cols = ucols(j)
+            r, cols = urows(j), ucols(j)
 
             @pl.when(b == mir)
             def _():
                 pair_send(b, j).wait_recv()
-                q2[:, cols] = (part2[b, :, cols].astype(F32) + got2[b, :, cols].astype(F32)).astype(BF16)
+                q2[r, cols] = (part2[b, r, cols].astype(F32) + got2[b, r, cols].astype(F32)).astype(BF16)
                 cross(j).start()
 
         def outer_stat(d):
             return remote(st2.at[0], finin.at[me], fs_, fr, {"fs": po, "tp": lax.rem(me + d, T)})
 
-        def finish(j):
-            pair_send(me, j).wait_recv()
-            cross(j).wait_recv()
-            cols = ucols(j)
-            for slot in range(2):
-                r = span_of(slot)
-                second = firsts[me, slot, :, cols].astype(F32) + part2[me, r, cols].astype(F32)
-                second = second + got2[me, r, cols].astype(F32) + q2in[r, cols].astype(F32)
-                if slot == 0:
-                    secb[:, cols] = second.astype(BF16)
-                    result(cols, po).start()
-                else:
-                    sec[:, cols] = second
-                total = jnp.sum(second * second, axis=1, keepdims=True)
-                if j > 0:
-                    total = total + ssq[r, :]
-                if j < 2:
-                    ssq[r, :] = total
-                    continue
-                st2[slot] = across_lanes(total, total)
-                if slot == 0:
-                    for d in range(T):
-                        outer_stat(d).start()
-                else:
-                    sg2[me] = st2[1]
-                    for d in range(1, T):
-                        stat(2, st2.at[1], sg2.at[me], d).start()
+        def finish(b, j):
+            @pl.when(b == me)
+            def _():
+                pair_send(me, j).wait_recv()
+                cross(j).wait_recv()
+                cols = ucols(j)
+                for slot in (0, 1) if j < 2 else (j - 2,):
+                    r = span_of(slot)
+                    second = firsts[me, slot, :, cols].astype(F32) + part2[me, r, cols].astype(F32)
+                    second = second + got2[me, r, cols].astype(F32) + q2in[r, cols].astype(F32)
+                    total = jnp.sum(second * second, axis=1, keepdims=True)
+                    if j > 0:
+                        total = total + ssq[r, :]
+                    if slot == 0:
+                        secb[:, cols] = second.astype(BF16)
+                        result(cols, po).start()
+                    else:
+                        sec[:, cols] = second
+                    if j < 2:
+                        ssq[r, :] = total
+                        continue
+                    st2[slot] = across_lanes(total, total)
+                    if slot == 0:
+                        for d in range(T):
+                            outer_stat(d).start()
+                    else:
+                        sg2[me] = st2[1]
+                        for d in range(1, T):
+                            stat(2, st2.at[1], sg2.at[me], d).start()
 
         own[DOWN].wait()
+        relay_mid(DOWN, 1)
         wait_mid(DOWN, 0, 2)
         wait_mid(DOWN, 0, 3)
         down(pi, 0)
         down(f, 0)
+        relay_y(DOWN, 1, 0)
         relay_mid(DOWN, 2)
         combine(pi, 0)
-        relay_y(DOWN, 1, 0)
+        down(f, 1)
         combine(f, 0)
         wait_y_down(0, 1)
         down(pi, 1)
-        down(f, 1)
         relay_mid(DOWN, 3)
         mid_direct(2).start()
         mid_direct(3).start()
-        combine(pi, 1)
         relay_y(DOWN, 1, 1)
         combine(f, 1)
+        combine(pi, 1)
         down(po, 0)
         down(f, 2)
+        down(f, 3)
         relay_y(DOWN, 1, 2)
         combine(po, 0)
         combine(f, 2)
+        combine(f, 3)
+        relay_y(DOWN, 1, 3)
         wait_y_down(1, 1)
         down(fo, 1)
-        relay_y(DOWN, 1, 3)
         down(fo, 0)
+        for j in range(4):
+            finish(f, j)
         combine(fo, 1)
         combine(fo, 0)
-        wait_z(DOWN)
+        wait_z_down(1)
         down(po, 1)
+        finish(pi, 0)
+        finish(po, 0)
+        combine(po, 1)
+        finish(pi, 1)
+        wait_z_down(2)
         down(po, 2)
-        combine(po, 1)
+        down(po, 3)
         wait_direct()
         down(pi, 2)
         wait_y_down(1, 2)
         down(fo, 2)
         combine(po, 2)
         combine(pi, 2)
+        down(pi, 3)
+        down(fo, 3)
         combine(fo, 2)
-        finish(0)
-        finish(1)
-        finish(2)
+        combine(po, 3)
+        combine(pi, 3)
+        combine(fo, 3)
+        finish(po, 1)
+        finish(fo, 0)
+        finish(fo, 1)
+        for j in (2, 3):
+            for b in (po, pi, fo):
+                finish(b, j)
         arrived(sg2.at[0:3], sts.at[2], str_.at[2])
         table = down_rows(sum(sg2[t] for t in range(T)))
         scale = lax.rsqrt(table[:, 0:1] / width + EPS)
@@ -914,8 +948,8 @@
         def sent(ref, sem):
             remote(ref, ref, sem, sem, {"fs": f}).wait_send()
 
-        all_sent(ms, 4)
-        all_sent(ys, 3)
+        all_sent(ms, 8)
+        all_sent(ys, 7)
         sent(bufs[DOWN].at[f, :, ucols(2)], md.at[0])
         for slot in range(2):
             sent(xg.at[0:3, slot], ags.at[0, slot])
@@ -945,7 +979,7 @@
     V = pltpu.VMEM
     out = pl.pallas_call(
         functools.partial(fast_kernel, length),
-        out_shape=jax.ShapeDtypeStruct((count, dt), BF16),
+        out_shape=pltpu.VMEM((count, dt), BF16),
         in_specs=[hbm] * 12,
         out_specs=vmem,
         scratch_shapes=[
@@ -986,7 +1020,7 @@
             dma((6,)),
             dma((3,)),
             dma((sum(PIECES),)),
-            dma((6,)),
+            dma((7,)),
             dma((3,)),
             dma((2, sum(PIECES))),
             dma((2,)),
@@ -1001,9 +1035,9 @@
             dma((2,)),
             dma((2, 2)),
             dma(()),
-            dma((2, 3)),
+            dma((2, 4)),
             dma(()),
-            dma((3,)),
+            dma((4,)),
             dma(()),
             dma(()),
             dma(()),

time: 113 us -> 114 us (level)
  Pallas kernels: 111 us -> 113 us
    pallas_call x1, Pallas kernels: 111 us -> 113 us  [fast_body(): pl.pallas_call(functools.partial(fast_kernel, length), out_shape=pltpu.VM...]
where the time goes in v4:
time: 114 us
  Pallas kernels  113 us (99%)
    pallas_call x1, Pallas kernels, fast_body(): pl.pallas_call(functools.partial(fast_kernel, length), out_shape=pltpu.VM...  113 us

profile of v4, /device:TPU:0, one launch (start us, length us, event | category | flops | bytes accessed | tf_op | source)
XLA Modules:
  0.0 113.6 jit_solution(16384017051086235394)
XLA Ops:
  0.0 112.9 %block.1 = bf16[256,512]{1,0:T(8,128)(2,1)S(1)} custom-call(bf16[256,512]{1,0:T(8,128)(2,1)} %bitcast.7, f32[1,2048]{1,0:T(1,128)} %bitcast.8, f32[31,512]{1,0:T(8,128)} %cw_hbm.1, f32[1,512]{1,0:T(1,128)} %bitcast.10, f32[1,2048]{1,0:T(1,128)} %bitcast.9, f32[1,512]{1,0:T(1,128)} %bitcast.11, bf16[512,512]{1,0:T(8,128)(2,1)} %wv_ref.1, ...), custom_call_target="tpu_custom_call" | custom-call | tf_op jit(solution)/shard_map/block/pallas_call | solution.py:980
  112.9 0.7 copy.14

commit v5 on v4

--- a/solution.py
+++ b/solution.py
@@ -434,10 +434,12 @@
     def ucols(j):
         if j == 0:
             return pl.ds(pl.multiple_of(rep * hn, hn), hn)
+        if j > 3:
+            return pl.ds(pl.multiple_of(rep * hn + (j - 4) * (hn // 2), hn // 2), hn // 2)
         return pl.ds(pl.multiple_of((1 - rep) * hn + min(j - 1, 1) * (hn // 2), hn // 2), hn // 2)
 
     def urows(j):
-        return slice(0, rows_all) if j < 2 else slice((j - 2) * count, (j - 1) * count)
+        return slice((j - 2) * count, (j - 1) * count) if j in (2, 3) else slice(0, rows_all)
 
     def result(cols, target):
         return remote(secb.at[:, cols], secin.at[:, cols], os_, orr, {"fs": target})
@@ -855,19 +857,19 @@
                 pair_send(me, j).wait_recv()
                 cross(j).wait_recv()
                 cols = ucols(j)
-                for slot in (0, 1) if j < 2 else (j - 2,):
+                for slot in (j - 2,) if j in (2, 3) else (0, 1):
                     r = span_of(slot)
                     second = firsts[me, slot, :, cols].astype(F32) + part2[me, r, cols].astype(F32)
                     second = second + got2[me, r, cols].astype(F32) + q2in[r, cols].astype(F32)
                     total = jnp.sum(second * second, axis=1, keepdims=True)
-                    if j > 0:
+                    if j not in (0, 4):
                         total = total + ssq[r, :]
                     if slot == 0:
                         secb[:, cols] = second.astype(BF16)
                         result(cols, po).start()
                     else:
                         sec[:, cols] = second
-                    if j < 2:
+                    if j not in (2, 3):
                         ssq[r, :] = total
                         continue
                     st2[slot] = across_lanes(total, total)
@@ -899,26 +901,27 @@
         combine(f, 1)
         combine(pi, 1)
         down(po, 0)
+        down(fo, 4)
+        relay_y(DOWN, 1, 2)
         down(f, 2)
         down(f, 3)
-        relay_y(DOWN, 1, 2)
         combine(po, 0)
+        combine(fo, 4)
+        relay_y(DOWN, 1, 3)
         combine(f, 2)
         combine(f, 3)
-        relay_y(DOWN, 1, 3)
+        down(fo, 5)
         wait_y_down(1, 1)
         down(fo, 1)
-        down(fo, 0)
-        for j in range(4):
-            finish(f, j)
-        combine(fo, 1)
-        combine(fo, 0)
+        finish(f, 0)
+        finish(pi, 0)
+        combine(fo, 5)
         wait_z_down(1)
         down(po, 1)
-        finish(pi, 0)
-        finish(po, 0)
+        combine(fo, 1)
+        finish(f, 1)
+        finish(pi, 1)
         combine(po, 1)
-        finish(pi, 1)
         wait_z_down(2)
         down(po, 2)
         down(po, 3)
@@ -934,11 +937,13 @@
         combine(po, 3)
         combine(pi, 3)
         combine(fo, 3)
+        finish(po, 0)
+        finish(fo, 4)
         finish(po, 1)
-        finish(fo, 0)
+        finish(fo, 5)
         finish(fo, 1)
         for j in (2, 3):
-            for b in (po, pi, fo):
+            for b in (f, po, pi, fo):
                 finish(b, j)
         arrived(sg2.at[0:3], sts.at[2], str_.at[2])
         table = down_rows(sum(sg2[t] for t in range(T)))
@@ -1035,9 +1040,9 @@
             dma((2,)),
             dma((2, 2)),
             dma(()),
-            dma((2, 4)),
+            dma((2, 6)),
             dma(()),
-            dma((4,)),
+            dma((6,)),
             dma(()),
             dma(()),
             dma(()),

time: 114 us -> 109 us (0.956)
  Pallas kernels: 113 us -> 108 us
    pallas_call x1, Pallas kernels: 113 us -> 108 us  [fast_body(): pl.pallas_call(functools.partial(fast_kernel, length), out_shape=pltpu.VM...]
where the time goes in v5:
time: 109 us
  Pallas kernels  108 us (99%)
    pallas_call x1, Pallas kernels, fast_body(): pl.pallas_call(functools.partial(fast_kernel, length), out_shape=pltpu.VM...  108 us

profile of v5, /device:TPU:0, one launch (start us, length us, event | category | flops | bytes accessed | tf_op | source)
XLA Modules:
  0.0 109.1 jit_solution(15557517188416607420)
XLA Ops:
  0.0 108.4 %block.1 = bf16[256,512]{1,0:T(8,128)(2,1)S(1)} custom-call(bf16[256,512]{1,0:T(8,128)(2,1)} %bitcast.7, f32[1,2048]{1,0:T(1,128)} %bitcast.8, f32[31,512]{1,0:T(8,128)} %cw_hbm.1, f32[1,512]{1,0:T(1,128)} %bitcast.10, f32[1,2048]{1,0:T(1,128)} %bitcast.9, f32[1,512]{1,0:T(1,128)} %bitcast.11, bf16[512,512]{1,0:T(8,128)(2,1)} %wv_ref.1, ...), custom_call_target="tpu_custom_call" | custom-call | tf_op jit(solution)/shard_map/block/pallas_call | solution.py:985
  108.4 0.7 copy.14

commit v6 on v5

--- a/solution.py
+++ b/solution.py
@@ -368,7 +368,7 @@
         tp_send(5, st2, sg2.at[me], d).wait_send()
 
 
-PIECES = (2, 2, 2, 2, 2, 4)
+PIECES = (2, 2, 2, 2, 2, 8)
 FIRST = tuple(sum(PIECES[:w]) for w in range(6))
 GROUP = (0, 0, 0, 1, 1, 2)
 
@@ -404,9 +404,9 @@
 
     def view(ref, w, h, c):
         if w == DOWN:
-            n, m = ref.shape[1] // 2, ref.shape[0] // 2
+            n, m = ref.shape[1] // 2, ref.shape[0] // 4
             k = n // 2
-            return ref.at[pl.ds((c % 2) * m, m), pl.ds(pl.multiple_of(h * n + (c // 2) * k, k), k)]
+            return ref.at[pl.ds((c % 4) * m, m), pl.ds(pl.multiple_of(h * n + (c // 4) * k, k), k)]
         n = ref.shape[0] // 2
         k = n // PIECES[w]
         return ref.at[pl.ds(pl.multiple_of(h * n + c * k, k), k), :]
@@ -418,7 +418,7 @@
 
     def zsend(w, hs, c):
         h = rep if hs == 0 else 1 - rep
-        sem = zr2.at[w + c // 2 if w == DOWN else w] if hs else zr.at[FIRST[w] + c]
+        sem = zr2.at[w + c // 4 if w == DOWN else w] if hs else zr.at[FIRST[w] + c]
         return remote(view(local[w], w, h, c), view(bufs[w].at[f], w, h, c), zs.at[GROUP[w]], sem, {"fs": near})
 
     def all_sent(sems, eighths):
@@ -476,10 +476,10 @@
             if item is None:
                 xsend().start()
             else:
-                for c in range(1 if item == (DOWN, 1) else 0, PIECES[item[0]]):
+                for c in range(PIECES[item[0]]):
                     zsend(item[0], item[1], c).start()
         xsend().wait_send()
-        all_sent(zs, 7)
+        all_sent(zs, 8)
         smalls[4].wait()
         remote(secb, secin, os_, orr, {"fs": near}).wait_recv()
         remote(finin, finin, fs_, fr, {"fs": near}).wait_recv()
@@ -523,19 +523,11 @@
 
         def y_fwd(w, k, c):
             ref = view(bufs[w].at[fo if k else pi], w, rep, c)
-            sem = yr.at[k, w + c // 2 if w == DOWN else w]
+            sem = yr.at[k, w + c // 4 if w == DOWN else w]
             return remote(ref, ref, ys.at[GROUP[w]], sem, {"rep": 1 - rep})
 
-        def y_outer():
-            ref = view(bufs[DOWN].at[po], DOWN, rep, 0)
-            return remote(ref, ref, ys.at[2], yr.at[0, 6], {"rep": 1 - rep})
-
         def wait_z_down(j):
-            if j == 1:
-                arrived(view(bufs[DOWN].at[po], DOWN, 1 - rep, 0), ys.at[2], yr.at[0, 6])
-                arrived(view(bufs[DOWN].at[po], DOWN, 1 - rep, 1), zs.at[2], zr2.at[DOWN])
-            else:
-                arrived(bufs[DOWN].at[po, :, ucols(2)], zs.at[2], zr2.at[DOWN + 1])
+            arrived(bufs[DOWN].at[po, :, ucols(j)], zs.at[2], zr2.at[DOWN + j - 1])
 
         def send_own(w):
             for c in range(PIECES[w]):
@@ -566,8 +558,10 @@
             ref = bufs[DOWN].at[fo if k else pi, :, ucols(j)]
             arrived(ref, ys.at[2], yr.at[k, DOWN + j - 1])
 
-        def wait_direct():
-            arrived(bufs[DOWN].at[pi, :, ucols(2)], md.at[0], md.at[1])
+        def wait_last():
+            m = bd.shape[1] // 2
+            arrived(bufs[DOWN].at[pi, 0:m, ucols(2)], ys.at[2], yr.at[0, 6])
+            arrived(bufs[DOWN].at[pi, m:2 * m, ucols(2)], md.at[0], md.at[1])
 
         def ag(p, buf, slot, kind):
             ref = buf.at[mir if kind == 2 else me, slot]
@@ -586,7 +580,7 @@
         def ag_finish(p, buf, slot):
             arrived(buf.at[0:2, slot], ags.at[p, slot], agr.at[p, slot, 0])
 
-        block = chunk_of(count, 16)
+        block = chunk_of(count, 32)
 
         def norm_rows(src, slot, gain):
             def step(i, _):
@@ -769,43 +763,46 @@
         activate(0)
         project(0)
         activate(1)
-        relay_mid(GA, 0)
         project(1)
         pair_sum(0)
         relay_y(GA, 0, 1)
+        relay_mid(GA, 0)
         pair_sum(1)
+        relay_y(UP, 0, 0)
         relay_mid(GA, 1)
-        relay_y(UP, 0, 0)
+        relay_y(UP, 0, 1)
         finish_first(0)
         relay_mid(UP, 0)
-        relay_y(UP, 0, 1)
+        relay_y(GA, 1, 0)
+        finish_first(1)
         relay_mid(UP, 1)
         send_own(DOWN)
-        relay_y(GA, 1, 0)
-        finish_first(1)
+        mid_direct(6).start()
         relay_y(GA, 1, 1)
+        relay_y(UP, 1, 0)
         ag_forward(1, firsts, 0)
-        relay_y(UP, 1, 0)
         ag_finish(1, firsts, 0)
         norm_rows(firsts, 0, mg_ref)
+        relay_y(UP, 1, 1)
         ag_forward(1, firsts, 1)
-        relay_y(UP, 1, 1)
         ag_finish(1, firsts, 1)
         relay_y(DOWN, 0, 0)
+        relay_y(DOWN, 0, 1)
         norm_rows(firsts, 1, mg_ref)
-        relay_y(DOWN, 0, 1)
+        relay_y(DOWN, 0, 2)
+        relay_y(DOWN, 0, 3)
 
         nf = chunk_of(ff, 256)
 
-        def s5(w, keep):
+        def s5(w, shards, keep):
             def step(c, _):
                 cols = pl.ds(pl.multiple_of(c * nf, nf), nf)
-                value = sum(jnp.dot(rows[t], bufs[w][t, :, cols], preferred_element_type=F32) for t in range(T))
+                value = sum(jnp.dot(rows[t], bufs[w][t, :, cols], preferred_element_type=F32) for t in shards)
                 if keep:
-                    accs[:, cols] = value
+                    accs[w - GA, :, cols] = value
                 else:
-                    gate = accs[:, cols]
-                    hid[:, cols] = (gate * jax.nn.sigmoid(gate) * value).astype(BF16)
+                    gate = accs[0, :, cols]
+                    hid[:, cols] = (gate * jax.nn.sigmoid(gate) * (value + accs[1, :, cols])).astype(BF16)
                 return 0
             lax.fori_loop(0, ff // nf, step, 0)
 
@@ -814,13 +811,16 @@
         wait_y(GA, 0)
         wait_y(GA, 1)
         wait_z(GA)
-        s5(GA, True)
+        s5(GA, (f, pi, po, fo), True)
         relay_mid(DOWN, 0)
-        y_outer().start()
         wait_y(UP, 0)
         wait_z(UP)
+        s5(UP, (f, pi, po), True)
+        relay_mid(DOWN, 1)
+        relay_y(DOWN, 0, 4)
+        relay_y(DOWN, 0, 5)
         wait_y(UP, 1)
-        s5(UP, False)
+        s5(UP, (fo,), False)
 
         def pair_send(b, j):
             at = (b, urows(j), ucols(j))
@@ -848,8 +848,8 @@
                 q2[r, cols] = (part2[b, r, cols].astype(F32) + got2[b, r, cols].astype(F32)).astype(BF16)
                 cross(j).start()
 
-        def outer_stat(d):
-            return remote(st2.at[0], finin.at[me], fs_, fr, {"fs": po, "tp": lax.rem(me + d, T)})
+        def outer_stat(t):
+            return remote(st2.at[0], finin.at[me], fs_, fr, {"fs": po, "tp": t})
 
         def finish(b, j):
             @pl.when(b == me)
@@ -866,50 +866,57 @@
                         total = total + ssq[r, :]
                     if slot == 0:
                         secb[:, cols] = second.astype(BF16)
-                        result(cols, po).start()
                     else:
                         sec[:, cols] = second
                     if j not in (2, 3):
                         ssq[r, :] = total
-                        continue
-                    st2[slot] = across_lanes(total, total)
+                    else:
+                        st2[slot] = across_lanes(total, total)
+                    if j == 2:
+                        for t in (mir, dia, me, sib):
+                            outer_stat(t).start()
+                    if j == 3:
+                        sg2[me] = st2[1]
+                        for d in (2, 1, 3):
+                            stat(2, st2.at[1], sg2.at[me], d).start()
                     if slot == 0:
-                        for d in range(T):
-                            outer_stat(d).start()
-                    else:
-                        sg2[me] = st2[1]
-                        for d in range(1, T):
-                            stat(2, st2.at[1], sg2.at[me], d).start()
+                        result(cols, po).start()
 
         own[DOWN].wait()
-        relay_mid(DOWN, 1)
-        wait_mid(DOWN, 0, 2)
-        wait_mid(DOWN, 0, 3)
+        for c in range(6, 8):
+            wait_mid(DOWN, 0, c)
         down(pi, 0)
         down(f, 0)
-        relay_y(DOWN, 1, 0)
         relay_mid(DOWN, 2)
+        relay_mid(DOWN, 3)
         combine(pi, 0)
         down(f, 1)
         combine(f, 0)
         wait_y_down(0, 1)
         down(pi, 1)
-        relay_mid(DOWN, 3)
-        mid_direct(2).start()
-        mid_direct(3).start()
+        relay_mid(DOWN, 4)
+        relay_mid(DOWN, 5)
+        relay_y(DOWN, 1, 0)
         relay_y(DOWN, 1, 1)
         combine(f, 1)
         combine(pi, 1)
+        down(f, 2)
+        down(f, 3)
+        relay_mid(DOWN, 6)
+        relay_mid(DOWN, 7)
+        mid_direct(7).start()
+        relay_y(DOWN, 1, 2)
+        relay_y(DOWN, 1, 3)
         down(po, 0)
         down(fo, 4)
-        relay_y(DOWN, 1, 2)
-        down(f, 2)
-        down(f, 3)
+        relay_y(DOWN, 1, 4)
+        relay_y(DOWN, 1, 5)
+        combine(f, 2)
+        combine(f, 3)
         combine(po, 0)
         combine(fo, 4)
-        relay_y(DOWN, 1, 3)
-        combine(f, 2)
-        combine(f, 3)
+        relay_y(DOWN, 1, 6)
+        relay_y(DOWN, 1, 7)
         down(fo, 5)
         wait_y_down(1, 1)
         down(fo, 1)
@@ -925,7 +932,8 @@
         wait_z_down(2)
         down(po, 2)
         down(po, 3)
-        wait_direct()
+        finish(po, 0)
+        wait_last()
         down(pi, 2)
         wait_y_down(1, 2)
         down(fo, 2)
@@ -937,7 +945,6 @@
         combine(po, 3)
         combine(pi, 3)
         combine(fo, 3)
-        finish(po, 0)
         finish(fo, 4)
         finish(po, 1)
         finish(fo, 5)
@@ -955,7 +962,7 @@
 
         all_sent(ms, 8)
         all_sent(ys, 7)
-        sent(bufs[DOWN].at[f, :, ucols(2)], md.at[0])
+        sent(bufs[DOWN].at[f, 0:bd.shape[1] // 2, ucols(2)], md.at[0])
         for slot in range(2):
             sent(xg.at[0:3, slot], ags.at[0, slot])
             sent(firsts.at[0:3, slot], ags.at[1, slot])
@@ -1007,7 +1014,7 @@
             V((2, count, dt), BF16),
             V((T, 2, count, dt), BF16),
             V((rows_all, ff), BF16),
-            V((rows_all, ff), F32),
+            V((2, rows_all, ff), F32),
             V((T, rows_all, dt), BF16),
             V((T, rows_all, dt), BF16),
             V((rows_all, dt), BF16),

time: 109 us -> 108 us (level)
    pallas_call x1, Pallas kernels: 108 us -> 107 us  [fast_body(): pl.pallas_call(functools.partial(fast_kernel, length), out_shape=pltpu.VM...]
where the time goes in v6:
time: 108 us
  Pallas kernels  107 us (99%)
    pallas_call x1, Pallas kernels, fast_body(): pl.pallas_call(functools.partial(fast_kernel, length), out_shape=pltpu.VM...  107 us

profile of v6, /device:TPU:0, one launch (start us, length us, event | category | flops | bytes accessed | tf_op | source)
XLA Modules:
  0.0 107.7 jit_solution(8793194053321730420)
XLA Ops:
  0.0 107.0 %block.1 = bf16[256,512]{1,0:T(8,128)(2,1)S(1)} custom-call(bf16[256,512]{1,0:T(8,128)(2,1)} %bitcast.7, f32[1,2048]{1,0:T(1,128)} %bitcast.8, f32[31,512]{1,0:T(8,128)} %cw_hbm.1, f32[1,512]{1,0:T(1,128)} %bitcast.10, f32[1,2048]{1,0:T(1,128)} %bitcast.9, f32[1,512]{1,0:T(1,128)} %bitcast.11, bf16[512,512]{1,0:T(8,128)(2,1)} %wv_ref.1, ...), custom_call_target="tpu_custom_call" | custom-call | tf_op jit(solution)/shard_map/block/pallas_call | solution.py:992
  107.0 0.7 copy.14

commit v7 on v6

--- a/solution.py
+++ b/solution.py
@@ -464,13 +464,12 @@
 
     @pl.when(outer)
     def _():
-        for t in range(T):
-            greet(fs=near, tp=t)
+        greet(fs=near)
         smalls[4].start()
-        pl.semaphore_wait(barrier, T)
+        pl.semaphore_wait(barrier, 1)
         order = [
             (VAL, 0), (GATE, 0), None, (CVO, 0), (VAL, 1), (GATE, 1), (CVO, 1),
-            (GA, 0), (UP, 0), (GA, 1), (UP, 1), (DOWN, 0), (DOWN, 1),
+            (GA, 0), (UP, 0), (GA, 1),
         ]
         for item in order:
             if item is None:
@@ -478,6 +477,14 @@
             else:
                 for c in range(PIECES[item[0]]):
                     zsend(item[0], item[1], c).start()
+        zsend(UP, 1, 0).start()
+        zsend(DOWN, 0, 0).start()
+        zsend(DOWN, 0, 1).start()
+        zsend(UP, 1, 1).start()
+        for c in range(2, PIECES[DOWN]):
+            zsend(DOWN, 0, c).start()
+        for c in range(PIECES[DOWN]):
+            zsend(DOWN, 1, c).start()
         xsend().wait_send()
         all_sent(zs, 8)
         smalls[4].wait()
@@ -489,11 +496,10 @@
 
     @pl.when(jnp.logical_not(outer))
     def _():
-        for t in range(T):
-            greet(fs=po, tp=t)
+        greet(fs=po)
         greet(fs=pi)
         greet(rep=1 - rep)
-        for t in (sib, mir, dia):
+        for t in (sib, mir):
             greet(tp=t)
         own = [pltpu.make_async_copy(local[w], bufs[w].at[f], own_sem.at[w]) for w in range(6)]
         load_x = pltpu.make_async_copy(x_ref, xg.at[me, 1], small.at[5])
@@ -502,7 +508,7 @@
             copy.start()
         for copy in own:
             copy.start()
-        pl.semaphore_wait(barrier, T + 5)
+        pl.semaphore_wait(barrier, 5)
 
         def arrived(ref, send, recv):
             remote(ref, ref, send, recv, {"fs": f}).wait_recv()
@@ -811,16 +817,16 @@
         wait_y(GA, 0)
         wait_y(GA, 1)
         wait_z(GA)
+        relay_mid(DOWN, 0)
         s5(GA, (f, pi, po, fo), True)
-        relay_mid(DOWN, 0)
+        relay_mid(DOWN, 1)
         wait_y(UP, 0)
-        wait_z(UP)
-        s5(UP, (f, pi, po), True)
-        relay_mid(DOWN, 1)
+        s5(UP, (f, pi), True)
         relay_y(DOWN, 0, 4)
         relay_y(DOWN, 0, 5)
+        wait_z(UP)
         wait_y(UP, 1)
-        s5(UP, (fo,), False)
+        s5(UP, (po, fo), False)
 
         def pair_send(b, j):
             at = (b, urows(j), ucols(j))

time: 108 us -> 108 us (level)
  no operation moved by 1% of the time
where the time goes in v7:
time: 108 us
  Pallas kernels  107 us (99%)
    pallas_call x1, Pallas kernels, fast_body(): pl.pallas_call(functools.partial(fast_kernel, length), out_shape=pltpu.VM...  107 us

profile of v7, /device:TPU:0, one launch (start us, length us, event | category | flops | bytes accessed | tf_op | source)
XLA Modules:
  0.0 107.7 jit_solution(5451463456436958256)
XLA Ops:
  0.0 107.0 %block.1 = bf16[256,512]{1,0:T(8,128)(2,1)S(1)} custom-call(bf16[256,512]{1,0:T(8,128)(2,1)} %bitcast.7, f32[1,2048]{1,0:T(1,128)} %bitcast.8, f32[31,512]{1,0:T(8,128)} %cw_hbm.1, f32[1,512]{1,0:T(1,128)} %bitcast.10, f32[1,2048]{1,0:T(1,128)} %bitcast.9, f32[1,512]{1,0:T(1,128)} %bitcast.11, bf16[512,512]{1,0:T(8,128)(2,1)} %wv_ref.1, ...), custom_call_target="tpu_custom_call" | custom-call | tf_op jit(solution)/shard_map/block/pallas_call | solution.py:998
  107.0 0.7 copy.14

commit v8 on v7

--- a/solution.py
+++ b/solution.py
@@ -783,7 +783,6 @@
         finish_first(1)
         relay_mid(UP, 1)
         send_own(DOWN)
-        mid_direct(6).start()
         relay_y(GA, 1, 1)
         relay_y(UP, 1, 0)
         ag_forward(1, firsts, 0)
@@ -910,6 +909,7 @@
         down(f, 3)
         relay_mid(DOWN, 6)
         relay_mid(DOWN, 7)
+        mid_direct(6).start()
         mid_direct(7).start()
         relay_y(DOWN, 1, 2)
         relay_y(DOWN, 1, 3)
@@ -932,24 +932,24 @@
         wait_z_down(1)
         down(po, 1)
         combine(fo, 1)
+        wait_last()
+        down(pi, 2)
+        down(pi, 3)
         finish(f, 1)
         finish(pi, 1)
         combine(po, 1)
         wait_z_down(2)
         down(po, 2)
         down(po, 3)
+        combine(pi, 2)
+        combine(pi, 3)
         finish(po, 0)
-        wait_last()
-        down(pi, 2)
         wait_y_down(1, 2)
         down(fo, 2)
         combine(po, 2)
-        combine(pi, 2)
-        down(pi, 3)
         down(fo, 3)
         combine(fo, 2)
         combine(po, 3)
-        combine(pi, 3)
         combine(fo, 3)
         finish(fo, 4)
         finish(po, 1)

time: 108 us -> 107 us (level)
  no operation moved by 1% of the time
where the time goes in v8:
time: 107 us
  Pallas kernels  107 us (100%)
    pallas_call x1, Pallas kernels, fast_body(): pl.pallas_call(functools.partial(fast_kernel, length), out_shape=pltpu.VM...  107 us

profile of v8, /device:TPU:0, one launch (start us, length us, event | category | flops | bytes accessed | tf_op | source)
XLA Modules:
  0.0 107.3 jit_solution(5648870785379668045)
XLA Ops:
  0.0 106.5 %block.1 = bf16[256,512]{1,0:T(8,128)(2,1)S(1)} custom-call(bf16[256,512]{1,0:T(8,128)(2,1)} %bitcast.7, f32[1,2048]{1,0:T(1,128)} %bitcast.8, f32[31,512]{1,0:T(8,128)} %cw_hbm.1, f32[1,512]{1,0:T(1,128)} %bitcast.10, f32[1,2048]{1,0:T(1,128)} %bitcast.9, f32[1,512]{1,0:T(1,128)} %bitcast.11, bf16[512,512]{1,0:T(8,128)(2,1)} %wv_ref.1, ...), custom_call_target="tpu_custom_call" | custom-call | tf_op jit(solution)/shard_map/block/pallas_call | solution.py:998
  106.5 0.7 copy.14

commit v9 on v8

--- a/solution.py
+++ b/solution.py
@@ -418,7 +418,7 @@
 
     def zsend(w, hs, c):
         h = rep if hs == 0 else 1 - rep
-        sem = zr2.at[w + c // 4 if w == DOWN else w] if hs else zr.at[FIRST[w] + c]
+        sem = zr2.at[(c + 1 if c > 5 else w + c // 4) if w == DOWN else w] if hs else zr.at[FIRST[w] + c]
         return remote(view(local[w], w, h, c), view(bufs[w].at[f], w, h, c), zs.at[GROUP[w]], sem, {"fs": near})
 
     def all_sent(sems, eighths):
@@ -483,7 +483,7 @@
         zsend(UP, 1, 1).start()
         for c in range(2, PIECES[DOWN]):
             zsend(DOWN, 0, c).start()
-        for c in range(PIECES[DOWN]):
+        for c in (6, 7, 0, 1, 2, 3, 4, 5):
             zsend(DOWN, 1, c).start()
         xsend().wait_send()
         all_sent(zs, 8)
@@ -523,9 +523,12 @@
             return remote(ref, ref, ms.at[GROUP[w]], mr.at[1, FIRST[w] + c], {"fs": pi})
 
         def mid_direct(c):
-            return remote(
-                view(local[DOWN], DOWN, 1 - rep, c), view(bufs[DOWN].at[f], DOWN, 1 - rep, c), md.at[0], md.at[1], {"fs": pi}
-            )
+            ref = view(bufs[DOWN].at[po], DOWN, 1 - rep, c)
+            return remote(ref, ref, md.at[0], md.at[1], {"fs": pi})
+
+        def relay_direct(c):
+            arrived(view(bufs[DOWN].at[po], DOWN, 1 - rep, c), zs.at[2], zr2.at[c + 1])
+            mid_direct(c).start()
 
         def y_fwd(w, k, c):
             ref = view(bufs[w].at[fo if k else pi], w, rep, c)
@@ -533,7 +536,8 @@
             return remote(ref, ref, ys.at[GROUP[w]], sem, {"rep": 1 - rep})
 
         def wait_z_down(j):
-            arrived(bufs[DOWN].at[po, :, ucols(j)], zs.at[2], zr2.at[DOWN + j - 1])
+            n = bd.shape[1] // (1 if j == 1 else 2)
+            arrived(bufs[DOWN].at[po, 0:n, ucols(j)], zs.at[2], zr2.at[DOWN + j - 1])
 
         def send_own(w):
             for c in range(PIECES[w]):
@@ -566,8 +570,8 @@
 
         def wait_last():
             m = bd.shape[1] // 2
-            arrived(bufs[DOWN].at[pi, 0:m, ucols(2)], ys.at[2], yr.at[0, 6])
-            arrived(bufs[DOWN].at[pi, m:2 * m, ucols(2)], md.at[0], md.at[1])
+            arrived(bufs[DOWN].at[fo, 0:m, ucols(2)], ys.at[2], yr.at[1, 6])
+            arrived(bufs[DOWN].at[fo, m:2 * m, ucols(2)], md.at[0], md.at[1])
 
         def ag(p, buf, slot, kind):
             ref = buf.at[mir if kind == 2 else me, slot]
@@ -822,7 +826,8 @@
         wait_y(UP, 0)
         s5(UP, (f, pi), True)
         relay_y(DOWN, 0, 4)
-        relay_y(DOWN, 0, 5)
+        for c in range(5, 8):
+            relay_y(DOWN, 0, c)
         wait_z(UP)
         wait_y(UP, 1)
         s5(UP, (po, fo), False)
@@ -888,8 +893,6 @@
                         result(cols, po).start()
 
         own[DOWN].wait()
-        for c in range(6, 8):
-            wait_mid(DOWN, 0, c)
         down(pi, 0)
         down(f, 0)
         relay_mid(DOWN, 2)
@@ -909,21 +912,26 @@
         down(f, 3)
         relay_mid(DOWN, 6)
         relay_mid(DOWN, 7)
-        mid_direct(6).start()
-        mid_direct(7).start()
         relay_y(DOWN, 1, 2)
         relay_y(DOWN, 1, 3)
         down(po, 0)
         down(fo, 4)
+        relay_direct(6)
+        relay_direct(7)
         relay_y(DOWN, 1, 4)
         relay_y(DOWN, 1, 5)
         combine(f, 2)
         combine(f, 3)
         combine(po, 0)
         combine(fo, 4)
-        relay_y(DOWN, 1, 6)
-        relay_y(DOWN, 1, 7)
+        wait_y_down(0, 2)
+        down(pi, 2)
+        down(pi, 3)
+        wait_mid(DOWN, 1, 6)
+        wait_mid(DOWN, 1, 7)
         down(fo, 5)
+        combine(pi, 2)
+        combine(pi, 3)
         wait_y_down(1, 1)
         down(fo, 1)
         finish(f, 0)
@@ -933,24 +941,19 @@
         down(po, 1)
         combine(fo, 1)
         wait_last()
-        down(pi, 2)
-        down(pi, 3)
+        down(fo, 2)
         finish(f, 1)
         finish(pi, 1)
         combine(po, 1)
+        down(fo, 3)
         wait_z_down(2)
         down(po, 2)
+        combine(fo, 2)
         down(po, 3)
-        combine(pi, 2)
-        combine(pi, 3)
         finish(po, 0)
-        wait_y_down(1, 2)
-        down(fo, 2)
         combine(po, 2)
-        down(fo, 3)
-        combine(fo, 2)
+        combine(fo, 3)
         combine(po, 3)
-        combine(fo, 3)
         finish(fo, 4)
         finish(po, 1)
         finish(fo, 5)
@@ -1038,7 +1041,7 @@
             dma((6,)),
             dma((3,)),
             dma((sum(PIECES),)),
-            dma((7,)),
+            dma((9,)),
             dma((3,)),
             dma((2, sum(PIECES))),
             dma((2,)),

time: 107 us -> 108 us (level)
  no operation moved by 1% of the time
where the time goes in v9:
time: 108 us; the launch traced here: 107 us
  Pallas kernels  107 us (99%)
    pallas_call x1, Pallas kernels, fast_body(): pl.pallas_call(functools.partial(fast_kernel, length), out_shape=pltpu.VM...  107 us

profile of v9, /device:TPU:0, one launch (start us, length us, event | category | flops | bytes accessed | tf_op | source)
XLA Modules:
  0.0 107.4 jit_solution(5991395328487214725)
XLA Ops:
  0.0 106.7 %block.1 = bf16[256,512]{1,0:T(8,128)(2,1)S(1)} custom-call(bf16[256,512]{1,0:T(8,128)(2,1)} %bitcast.7, f32[1,2048]{1,0:T(1,128)} %bitcast.8, f32[31,512]{1,0:T(8,128)} %cw_hbm.1, f32[1,512]{1,0:T(1,128)} %bitcast.10, f32[1,2048]{1,0:T(1,128)} %bitcast.9, f32[1,512]{1,0:T(1,128)} %bitcast.11, bf16[512,512]{1,0:T(8,128)(2,1)} %wv_ref.1, ...), custom_call_target="tpu_custom_call" | custom-call | tf_op jit(solution)/shard_map/block/pallas_call | solution.py:1001
  106.7 0.7 copy.14

commit v10 on v8

--- a/solution.py
+++ b/solution.py
@@ -371,6 +371,7 @@
 PIECES = (2, 2, 2, 2, 2, 8)
 FIRST = tuple(sum(PIECES[:w]) for w in range(6))
 GROUP = (0, 0, 0, 1, 1, 2)
+SLOT = (0, 1, 2, 3, 0, 4)
 
 
 def fast_kernel(
@@ -416,10 +417,13 @@
     def greet(**target):
         pl.semaphore_signal(barrier, inc=1, device_id=target, device_id_type=MESH)
 
+    def source(w):
+        return bufs[w].at[f] if w == VAL else local[w]
+
     def zsend(w, hs, c):
         h = rep if hs == 0 else 1 - rep
         sem = zr2.at[w + c // 4 if w == DOWN else w] if hs else zr.at[FIRST[w] + c]
-        return remote(view(local[w], w, h, c), view(bufs[w].at[f], w, h, c), zs.at[GROUP[w]], sem, {"fs": near})
+        return remote(view(source(w), w, h, c), view(bufs[w].at[f], w, h, c), zs.at[GROUP[w]], sem, {"fs": near})
 
     def all_sent(sems, eighths):
         n = bd.shape[1] * eighths // 8
@@ -465,8 +469,11 @@
     @pl.when(outer)
     def _():
         greet(fs=near)
+        first = pltpu.make_async_copy(local[VAL], bufs[VAL].at[f], own_sem.at[VAL])
+        first.start()
         smalls[4].start()
         pl.semaphore_wait(barrier, 1)
+        first.wait()
         order = [
             (VAL, 0), (GATE, 0), None, (CVO, 0), (VAL, 1), (GATE, 1), (CVO, 1),
             (GA, 0), (UP, 0), (GA, 1),
@@ -515,7 +522,7 @@
 
         def mid_own(w, c):
             return remote(
-                view(local[w], w, rep, c), view(bufs[w].at[f], w, rep, c), ms.at[GROUP[w]], mr.at[0, FIRST[w] + c], {"fs": pi}
+                view(source(w), w, rep, c), view(bufs[w].at[f], w, rep, c), ms.at[GROUP[w]], mr.at[0, FIRST[w] + c], {"fs": pi}
             )
 
         def mid_fwd(w, c):
@@ -603,6 +610,7 @@
         def stat(k, src, dst, d):
             return remote(src, dst, sts.at[k], str_.at[k], {"tp": lax.rem(me + d, T)})
 
+        own[VAL].wait()
         send_own(VAL)
         send_own(GATE)
         load_x.wait()
@@ -661,7 +669,6 @@
                 return 0
             lax.fori_loop(0, chan // nc, step, 0)
 
-        own[VAL].wait()
         own[GATE].wait()
         s1(f, True, False)
         wait_y(VAL, 0)
@@ -829,11 +836,11 @@
 
         def pair_send(b, j):
             at = (b, urows(j), ucols(j))
-            return remote(part2.at[at], got2.at[at], ds_, dr.at[lax.rem(b // 2 + me // 2, 2), j], {"tp": sib})
+            return remote(part2.at[at], got2.at[at], ds_, dr.at[lax.rem(b // 2 + me // 2, 2), SLOT[j]], {"tp": sib})
 
         def cross(j):
             at = (urows(j), ucols(j))
-            return remote(q2.at[at], q2in.at[at], qs, qr.at[j], {"tp": mir})
+            return remote(q2.at[at], q2in.at[at], qs, qr.at[SLOT[j]], {"tp": mir})
 
         def down(b, j):
             r, cols = urows(j), ucols(j)
@@ -1053,9 +1060,9 @@
             dma((2,)),
             dma((2, 2)),
             dma(()),
-            dma((2, 6)),
+            dma((2, 5)),
             dma(()),
-            dma((6,)),
+            dma((5,)),
             dma(()),
             dma(()),
             dma(()),

time: 107 us -> 108 us (level)
  no operation moved by 1% of the time
where the time goes in v10:
time: 108 us
  Pallas kernels  107 us (99%)
    pallas_call x1, Pallas kernels, fast_body(): pl.pallas_call(functools.partial(fast_kernel, length), out_shape=pltpu.VM...  107 us

profile of v10, /device:TPU:0, one launch (start us, length us, event | category | flops | bytes accessed | tf_op | source)
XLA Modules:
  0.0 107.6 jit_solution(13278747953021791097)
XLA Ops:
  0.0 106.9 %block.1 = bf16[256,512]{1,0:T(8,128)(2,1)S(1)} custom-call(bf16[256,512]{1,0:T(8,128)(2,1)} %bitcast.7, f32[1,2048]{1,0:T(1,128)} %bitcast.8, f32[31,512]{1,0:T(8,128)} %cw_hbm.1, f32[1,512]{1,0:T(1,128)} %bitcast.10, f32[1,2048]{1,0:T(1,128)} %bitcast.9, f32[1,512]{1,0:T(1,128)} %bitcast.11, bf16[512,512]{1,0:T(8,128)(2,1)} %wv_ref.1, ...), custom_call_target="tpu_custom_call" | custom-call | tf_op jit(solution)/shard_map/block/pallas_call | solution.py:1005
  106.9 0.7 copy.14
